TPU v7x, 32 devices: a whole 2x2x4 slice. The times are simulated.
32 devices in a mesh: fs: 8 (over z, x), tp: 4 (over y, core).
Axes of the slice: x: 2, y: 2, z: 4, core: 2. Of those that a mesh axis runs over, the one named last changes fastest.
Arguments:
- tokens: bfloat16 [4096, 2048], P('fs', 'tp'), may hold values from -6 to 6
- pre_gain: float32 [2048], replicated, may hold values from 0.1 to 1.9
- pre_gate: float32 [2048, 2816], P('fs', 'tp'), may hold values from -0.125 to 0.125
- pre_up: float32 [2048, 2816], P('fs', 'tp'), may hold values from -0.125 to 0.125
- pre_down: float32 [2816, 2048], P('fs', 'tp'), may hold values from -0.109375 to 0.109375
- mix_gain: float32 [2048], replicated, may hold values from 0.1 to 1.9
- branch_proj: float32 [2048, 1024], P('fs', 'tp'), may hold values from -0.125 to 0.125
- gate_proj: float32 [2048, 1024], P('fs', 'tp'), may hold values from -0.125 to 0.125
- conv_taps: float32 [4, 1024], P(None, 'tp'), may hold values from -3 to 3
- retain_blocks: float32 [16, 64, 64], P('tp'), may hold values from -0.75 to 0.75
- admit_blocks: float32 [16, 64, 64], P('tp'), may hold values from -0.75 to 0.75
- decay_param: float32 [1024], P('tp'), may hold values from 5 to 8.5
- channel_gain: float32 [1024], replicated, may hold values from 0.1 to 1.9
- out_proj: float32 [1024, 2048], P('fs', 'tp'), may hold values from -0.1875 to 0.1875
- post_gain: float32 [2048], replicated, may hold values from 0.1 to 1.9
- post_gate: float32 [2048, 2816], P('fs', 'tp'), may hold values from -0.125 to 0.125
- post_up: float32 [2048, 2816], P('fs', 'tp'), may hold values from -0.125 to 0.125
- post_down: float32 [2816, 2048], P('fs', 'tp'), may hold values from -0.109375 to 0.109375
Outputs:
- layer_out: bfloat16 [4096, 2048], P('fs', 'tp')
All inputs are finite; a program needn't handle non-finite values.
Results may differ from a plain program's by a relative error of at most 0.012.
Values may be sent and summed in bfloat16 or wider, within the bound.
A program may use at most 64 MiB of HBM per device.

v0:
```python
import functools

import jax
import jax.numpy as jnp
from jax import lax
from jax.experimental import pallas as pl
from jax.experimental.pallas import tpu as pltpu
from jax.sharding import PartitionSpec as P

SEQ_LEN = 128


EPSILON = 1e-06
DECAY_SCALE = 8.0


def normalize(values, norm_gain):
    floats = values.astype(jnp.float32)
    scaled = floats * lax.rsqrt(jnp.mean(floats * floats, axis=-1, keepdims=True) + EPSILON)
    return (scaled * norm_gain).astype(jnp.bfloat16)


def widen(residual):
    return lax.all_gather(residual, "tp", axis=1, tiled=True)


def contract(operand, stacked):
    return jnp.dot(
        operand,
        lax.all_gather(stacked.astype(jnp.bfloat16), "fs", axis=0, tiled=True),
        preferred_element_type=jnp.float32,
    )


def feed_forward(residual, norm_gain, gate_matrix, up_matrix, down_matrix):
    normed = normalize(widen(residual), norm_gain)
    products = contract(normed, jnp.concatenate((gate_matrix, up_matrix), axis=1))
    split_at = gate_matrix.shape[1]
    hidden = (jax.nn.silu(products[:, :split_at]) * products[:, split_at:]).astype(jnp.bfloat16)
    all_hidden = lax.all_gather(hidden, "tp", axis=1, tiled=True)
    return (residual.astype(jnp.float32) + 0.5 * contract(all_hidden, down_matrix)).astype(
        jnp.bfloat16
    )


def shifted(values, distance, fill):
    row = lax.broadcasted_iota(jnp.int32, values.shape, 0)
    return jnp.where(row >= distance, pltpu.roll(values, distance, 0), fill)


def mix_sequence(branch, gate_act, taps, gates, sharpness):
    width = branch.shape[1]
    count = taps.shape[0]
    convolved = branch * taps[count - 1 : count]
    for back in range(1, count):
        convolved = convolved + shifted(branch, back, 0.0) * taps[count - 1 - back : count - back]
    convolved = convolved.astype(jnp.bfloat16)
    both = jax.nn.sigmoid(jnp.dot(convolved, gates, preferred_element_type=jnp.float32))
    log_keep = -DECAY_SCALE * both[:, :width] * sharpness
    keep = jnp.exp(log_keep)
    inject = (
        jnp.sqrt(jnp.tanh(-log_keep) * (1.0 + keep * keep))
        * both[:, width:]
        * convolved.astype(jnp.float32)
    )
    distance = 1
    while distance < branch.shape[0]:
        inject = keep * shifted(inject, distance, 0.0) + inject
        keep = keep * shifted(keep, distance, 1.0)
        distance *= 2
    return (inject * jax.nn.gelu(gate_act)).astype(jnp.bfloat16)


def mix_kernel(products_ref, taps_ref, gates_ref, sharp_ref, out_ref):
    width = out_ref.shape[1]
    out_ref[...] = mix_sequence(
        products_ref[:, :width],
        products_ref[:, width:],
        taps_ref[...],
        gates_ref[...],
        sharp_ref[...],
    )


def spread_blocks(blocks):
    count, size, _ = blocks.shape
    eye = jnp.eye(count, dtype=blocks.dtype)
    wide = eye[:, None, :, None] * blocks[:, :, None, :]
    return wide.reshape(count * size, count * size).astype(jnp.bfloat16)


def recurrent_mixer(
    residual,
    norm_gain,
    branch_matrix,
    gate_matrix,
    conv_taps,
    retain_blocks,
    admit_blocks,
    decay_param,
    channel_gain,
    out_matrix,
):
    normed = normalize(widen(residual), norm_gain)
    products = contract(normed, jnp.concatenate((branch_matrix, gate_matrix), axis=1))
    width = branch_matrix.shape[1]
    rows = residual.shape[0]
    gates = jnp.concatenate((spread_blocks(retain_blocks), spread_blocks(admit_blocks)), axis=1)
    sharpness = jax.nn.softplus(-decay_param)[None, :]
    whole = lambda array: pl.BlockSpec(array.shape, lambda i: (0, 0))
    mixed_rows = pl.pallas_call(
        mix_kernel,
        grid=(rows // SEQ_LEN,),
        in_specs=[
            pl.BlockSpec((SEQ_LEN, 2 * width), lambda i: (i, 0)),
            whole(conv_taps),
            whole(gates),
            whole(sharpness),
        ],
        out_specs=pl.BlockSpec((SEQ_LEN, width), lambda i: (i, 0)),
        out_shape=jax.ShapeDtypeStruct((rows, width), jnp.bfloat16),
        cost_estimate=pl.CostEstimate(
            flops=rows * width * 1200, bytes_accessed=rows * width * 10, transcendentals=0
        ),
    )(products, conv_taps, gates, sharpness)
    all_channels = lax.all_gather(mixed_rows, "tp", axis=1, tiled=True)
    mixed_normed = normalize(all_channels, channel_gain)
    return (residual.astype(jnp.float32) + contract(mixed_normed, out_matrix)).astype(jnp.bfloat16)


ROW_TILE = 256
MESH = pl.DeviceIdType.MESH


class Exchange:
    def __init__(self):
        self.sent = []

    def send(self, source, target, send_sem, recv_sem, device, condition=None):
        copy = pltpu.make_async_remote_copy(
            src_ref=source,
            dst_ref=target,
            send_sem=send_sem,
            recv_sem=recv_sem,
            device_id=device,
            device_id_type=MESH,
        )
        when(condition, copy.start)
        self.sent.append((copy, condition))

    def drain(self):
        for copy, condition in self.sent:
            when(condition, copy.wait_send)


def when(condition, action):
    if condition is None:
        action()
    else:
        pl.when(condition)(action)


def layer_kernel(fs_size, tp_size, *refs):
    (tokens, pre_gain, mix_gain, channel_gain, post_gain, taps, gates, sharpness) = refs[:8]
    shards = refs[8:16]
    out = refs[16]
    whole = refs[17:25]
    first, second, third, hidden_one, hidden_two, channels, normed = refs[25:32]
    recv_sem, line_sem, back_sem, pair_sem, keep_sem = refs[32:37]
    tp_recv, tp_peer, tp_own, tp_pass, token_sem = refs[37:42]

    f = lax.axis_index("fs")
    t = lax.axis_index("tp")
    x = lax.rem(f, 2)
    z = f // 2
    depth = fs_size // 2
    half = tp_size // 2
    across = {"fs": f + 1 - 2 * x}
    above = {"fs": lax.rem(f + 2, fs_size)}
    below = {"fs": lax.rem(f + fs_size - 2, fs_size)}
    has_above = z < depth - 1
    has_below = z > 0
    twin = t + 1 - 2 * lax.rem(t, 2)
    peers = [lax.rem(t + 2 * k, tp_size) for k in range(1, half)]
    links = Exchange()

    barrier = pltpu.get_barrier_semaphore()
    greeted = [(across, None), (above, has_above), (below, has_below), ({"tp": twin}, None)]
    greeted += [({"tp": peer}, None) for peer in peers]
    for device, condition in greeted:
        when(
            condition,
            functools.partial(
                pl.semaphore_signal, barrier, inc=1, device_id=device, device_id_type=MESH
            ),
        )
    line_ends = (z == 0).astype(jnp.int32) + (z == depth - 1).astype(jnp.int32)
    pl.semaphore_wait(barrier, len(greeted) - line_ends)

    def shard_at(p, owner):
        rows = shards[p].shape[0]
        return whole[p].at[pl.ds(pl.multiple_of(owner * rows, rows), rows)]

    def arrive(p, owner, condition=None):
        place = shard_at(p, owner)
        copy = pltpu.make_async_remote_copy(
            src_ref=place,
            dst_ref=place,
            send_sem=pair_sem.at[p, 0],
            recv_sem=recv_sem.at[p, owner],
            device_id=across,
            device_id_type=MESH,
        )
        when(condition, copy.wait_recv)

    def own_copy(p):
        return pltpu.make_async_copy(shards[p], shard_at(p, f), keep_sem.at[p])

    def launch(p):
        place, sem = shard_at(p, f), recv_sem.at[p, f]
        links.send(shards[p], place, line_sem.at[p, f], sem, above, has_above)
        links.send(shards[p], place, back_sem.at[p, 0], sem, below, has_below)
        links.send(shards[p], place, pair_sem.at[p, z], sem, across)
        own_copy(p).start()

    def launch_pair(p):
        owner = f + 1 - 2 * x
        arrive(p, owner)
        place, sem = shard_at(p, owner), recv_sem.at[p, owner]
        links.send(place, place, line_sem.at[p, owner], sem, above, has_above)
        links.send(place, place, back_sem.at[p, 1], sem, below, has_below)

    def relay(p, distance, column, cross):
        for sign, edge, there in ((-1, above, has_above), (1, below, has_below)):
            level = z + sign * distance
            exists = (level >= 0) & (level < depth)
            level = lax.rem(level + depth, depth)
            owner = level * 2 + column
            arrive(p, owner, exists)
            place, sem = shard_at(p, owner), recv_sem.at[p, owner]
            links.send(place, place, line_sem.at[p, owner], sem, edge, exists & there)
            if cross:
                links.send(place, place, pair_sem.at[p, level], sem, across, exists)

    count = len(shards)
    direct = (2,)

    def step(number):
        for p in range(count):
            if max(p - 1, 0) == number:
                launch(p)
        for p in range(count):
            if p in direct:
                if p + 1 == number:
                    launch_pair(p)
                if 1 <= number - p - 1 < depth:
                    relay(p, number - p - 1, 1 - x, False)
            if 1 <= number - p < depth:
                relay(p, number - p, x, p not in direct)

    def ready(p):
        own_copy(p).wait()
        if p not in direct:
            for level in range(depth):
                arrive(p, level * 2 + 1 - x)

    def spread(array, index):
        for k, peer in enumerate(peers):
            links.send(
                array.at[t], array.at[t], tp_peer.at[index, k], tp_recv.at[index, t], {"tp": peer}
            )
        links.send(
            array.at[t], array.at[t], tp_own.at[index], tp_recv.at[index, t], {"tp": twin}
        )

    def landed(array, index, slot):
        pltpu.make_async_remote_copy(
            src_ref=array.at[slot],
            dst_ref=array.at[slot],
            send_sem=tp_own.at[index],
            recv_sem=tp_recv.at[index, slot],
            device_id={"tp": twin},
            device_id_type=MESH,
        ).wait_recv()

    def collect(array, index):
        for k, peer in enumerate(peers):
            landed(array, index, peer)
            links.send(
                array.at[peer],
                array.at[peer],
                tp_pass.at[index, k],
                tp_recv.at[index, peer],
                {"tp": twin},
            )
        landed(array, index, twin)
        for k in range(1, half):
            landed(array, index, lax.rem(twin + 2 * k, tp_size))

    total_rows = tokens.shape[0]

    def tiles(size, body):
        def run(i, carry):
            body(pl.ds(pl.multiple_of(i * size, size), size))
            return carry

        lax.fori_loop(0, total_rows // size, run, 0)

    def norm_slots(array, gain):
        width = array.shape[2]
        features = width * tp_size

        def body(rows):
            parts = [array[s, rows, :].astype(jnp.float32) for s in range(tp_size)]
            squares = sum(jnp.sum(part * part, axis=-1, keepdims=True) for part in parts)
            scale = lax.rsqrt(squares / features + EPSILON)
            for s, part in enumerate(parts):
                at = slice(s * width, (s + 1) * width)
                normed[rows, at] = (part * scale * gain[:, at]).astype(jnp.bfloat16)

        tiles(64, body)

    def dot(left, right):
        return jnp.dot(left, right, preferred_element_type=jnp.float32)

    def gated(gate, up, hidden):
        features = gate.shape[1]
        width = hidden.shape[2]

        def turned(rows, matrix):
            return sum(
                lax.dot_general(
                    normed[rows, s * features : (s + 1) * features],
                    matrix[s * width : (s + 1) * width, :],
                    (((1,), (1,)), ((), ())),
                    preferred_element_type=jnp.float32,
                )
                for s in range(fs_size)
            )

        def body(rows):
            product = jax.nn.silu(turned(rows, gate)) * turned(rows, up)
            hidden[t, rows, :] = product.astype(jnp.bfloat16)

        tiles(ROW_TILE, body)

    def lower(hidden, down, residual, store):
        width = hidden.shape[2]

        def body(rows):
            total = sum(
                dot(hidden[s, rows, :], down[s * width : (s + 1) * width, :])
                for s in range(tp_size)
            )
            value = residual[t, rows, :].astype(jnp.float32) + 0.5 * total
            store(rows, value.astype(jnp.bfloat16))

        tiles(ROW_TILE, body)

    def mix(rows):
        width = channels.shape[2]
        products = dot(normed[rows, :], whole[3][...])
        channels[t, rows, :] = mix_sequence(
            products[:, :width], products[:, width:], taps[...], gates[...], sharpness[...]
        )

    def put(array):
        def store(rows, value):
            array[t, rows, :] = value

        return store

    def finish(rows, value):
        out[rows, :] = value

    def project(rows):
        width = channels.shape[2] * tp_size
        total = dot(normed[rows, :width], whole[4][...])
        third[t, rows, :] = (second[t, rows, :].astype(jnp.float32) + total).astype(jnp.bfloat16)

    local_tokens = pltpu.make_async_copy(tokens, first.at[t], token_sem)
    local_tokens.start()
    step(0)
    local_tokens.wait()
    spread(first, 0)
    step(1)
    step(2)
    collect(first, 0)
    norm_slots(first, pre_gain)
    step(3)
    step(4)
    step(5)
    ready(0)
    ready(1)
    gated(whole[0], whole[1], hidden_one)
    spread(hidden_one, 1)
    step(6)
    collect(hidden_one, 1)
    ready(2)
    lower(hidden_one, whole[2], first, put(second))
    spread(second, 2)
    step(7)
    collect(second, 2)
    norm_slots(second, mix_gain)
    ready(3)
    tiles(SEQ_LEN, mix)
    spread(channels, 3)
    step(8)
    collect(channels, 3)
    norm_slots(channels, channel_gain)
    ready(4)
    tiles(ROW_TILE, project)
    spread(third, 4)
    step(9)
    collect(third, 4)
    norm_slots(third, post_gain)
    for number in range(10, count + depth - 2):
        step(number)
    ready(5)
    ready(6)
    gated(whole[5], whole[6], hidden_two)
    spread(hidden_two, 5)
    for number in range(max(10, count + depth - 2), count + depth):
        step(number)
    collect(hidden_two, 5)
    ready(7)
    lower(hidden_two, whole[7], third, finish)
    links.drain()


def fused(
    fs_size,
    tp_size,
    tokens,
    pre_gain,
    pre_gate,
    pre_up,
    pre_down,
    mix_gain,
    branch_proj,
    gate_proj,
    conv_taps,
    retain_blocks,
    admit_blocks,
    decay_param,
    channel_gain,
    out_proj,
    post_gain,
    post_gate,
    post_up,
    post_down,
):
    half_type = lambda array: array.astype(jnp.bfloat16)
    shards = [
        half_type(pre_gate.T),
        half_type(pre_up.T),
        half_type(pre_down),
        jnp.concatenate((half_type(branch_proj), half_type(gate_proj)), axis=1),
        half_type(out_proj),
        half_type(post_gate.T),
        half_type(post_up.T),
        half_type(post_down),
    ]
    gates = jnp.concatenate((spread_blocks(retain_blocks), spread_blocks(admit_blocks)), axis=1)
    sharpness = jax.nn.softplus(-decay_param)[None, :]
    rows, width = tokens.shape
    hidden = pre_gate.shape[1]
    operands = [
        tokens,
        pre_gain[None],
        mix_gain[None],
        channel_gain[None],
        post_gain[None],
        conv_taps,
        gates,
        sharpness,
        *shards,
    ]
    dma = pltpu.SemaphoreType.DMA
    count = len(shards)
    stacked = lambda columns: pltpu.VMEM((tp_size, rows, columns), jnp.bfloat16)
    peers = max(tp_size // 2 - 1, 1)
    return pl.pallas_call(
        functools.partial(layer_kernel, fs_size, tp_size),
        out_shape=jax.ShapeDtypeStruct(tokens.shape, tokens.dtype),
        in_specs=[pl.BlockSpec(memory_space=pltpu.VMEM)] * len(operands),
        out_specs=pl.BlockSpec(memory_space=pltpu.VMEM),
        scratch_shapes=[
            *(pltpu.VMEM((fs_size * s.shape[0], s.shape[1]), jnp.bfloat16) for s in shards),
            stacked(width),
            stacked(width),
            stacked(width),
            stacked(hidden),
            stacked(hidden),
            stacked(branch_proj.shape[1]),
            pltpu.VMEM((rows, width * tp_size), jnp.bfloat16),
            dma((count, fs_size)),
            dma((count, fs_size)),
            dma((count, 2)),
            dma((count, fs_size // 2)),
            dma((count,)),
            dma((6, tp_size)),
            dma((6, peers)),
            dma((6,)),
            dma((6, peers)),
            dma,
        ],
        compiler_params=pltpu.CompilerParams(
            collective_id=0, has_side_effects=True, vmem_limit_bytes=62 * 2**20
        ),
    )(*operands)


def fits_fused(fs_size, tp_size, arrays):
    shards = [a for i, a in enumerate(arrays) if i in (2, 3, 4, 6, 7, 13, 15, 16, 17)]
    rows_fit = all(a.shape[0] % 16 == 0 for a in shards)
    lanes_fit = all(arrays[i].shape[1] % 128 == 0 for i in (0, 6, 7))
    tiles_fit = arrays[0].shape[0] % ROW_TILE == 0 and arrays[2].shape[1] % 16 == 0
    turned_fit = all(arrays[i].shape[0] % 128 == 0 for i in (2, 3, 15, 16))
    return (
        rows_fit
        and lanes_fit
        and tiles_fit
        and turned_fit
        and fs_size % 2 == 0
        and 4 <= fs_size <= 16
        and tp_size % 2 == 0
    )


def local(
    tokens,
    pre_gain,
    pre_gate,
    pre_up,
    pre_down,
    mix_gain,
    branch_proj,
    gate_proj,
    conv_taps,
    retain_blocks,
    admit_blocks,
    decay_param,
    channel_gain,
    out_proj,
    post_gain,
    post_gate,
    post_up,
    post_down,
):
    after_pre = feed_forward(tokens, pre_gain, pre_gate, pre_up, pre_down)
    after_mix = recurrent_mixer(
        after_pre,
        mix_gain,
        branch_proj,
        gate_proj,
        conv_taps,
        retain_blocks,
        admit_blocks,
        decay_param,
        channel_gain,
        out_proj,
    )
    return feed_forward(after_mix, post_gain, post_gate, post_up, post_down)


def solution(mesh):
    placed = (
        P("fs", "tp"),
        P(),
        P("fs", "tp"),
        P("fs", "tp"),
        P("fs", "tp"),
        P(),
        P("fs", "tp"),
        P("fs", "tp"),
        P(None, "tp"),
        P("tp", None, None),
        P("tp", None, None),
        P("tp"),
        P(),
        P("fs", "tp"),
        P(),
        P("fs", "tp"),
        P("fs", "tp"),
        P("fs", "tp"),
    )
    fs_size, tp_size = mesh.shape["fs"], mesh.shape["tp"]

    def layer(*arrays):
        if fits_fused(fs_size, tp_size, arrays):
            return fused(fs_size, tp_size, *arrays)
        return local(*arrays)

    return jax.shard_map(
        layer, mesh=mesh, in_specs=placed, out_specs=P("fs", "tp"), check_vma=False
    )
```

profile of v0, /device:TPU:1, one launch (start us, length us, event | category | flops | bytes accessed | tf_op | source)
XLA Modules:
  0.0 242.8 jit_solution(15372791506773099561)
XLA Ops:
  0.0 0.0 copy-start.6
  0.0 0.0 copy-start
  0.0 1.3 compare_select_fusion
  1.3 1.0 convert_element_type.67
  2.3 0.0 copy-done.6
  2.3 0.0 copy-start.1
  2.3 1.7 convert_element_type.69.refs_12_
  4.0 0.0 copy-done
  4.0 0.8 convert_element_type.66.refs_10_
  4.8 0.0 copy-done.1
  4.8 0.0 copy-start.7
  4.8 0.0 copy-start.8
  4.8 0.8 convert_element_type.74.refs_15_
  5.6 0.1 copy-done.7
  5.7 0.2 copy-done.8
  5.9 0.3 multiply_convert_fusion.1
  6.2 0.2 convert_element_type.59
  6.4 0.0 copy-start.2
  6.4 0.0 copy-start.3
  6.4 0.2 convert_element_type.61
  6.6 0.8 pad_maximum_fusion
  7.5 0.0 copy-done.2
  7.5 0.4 copy-done.3
  7.9 0.0 copy-start.4
  7.9 0.0 copy-start.5
  7.9 0.9 convert_bitcast_fusion.2
  8.8 0.4 copy-done.4
  9.3 0.2 copy-done.5
  9.5 0.9 convert_bitcast_fusion
  10.4 230.5 %shard_map.172 = bf16[512,512]{1,0:T(8,128)(2,1)} custom-call(bf16[512,512]{1,0:T(8,128)(2,1)} %refs_0_.1, f32[1,2048]{1,0:T(1,128)} %bitcast.13, f32[1,2048]{1,0:T(1,128)} %bitcast.14, f32[1,1024]{1,0:T(1,128)} %bitcast.17, f32[1,2048]{1,0:T(1,128)} %bitcast.15, f32[4,256]{1,0:T(4,128)} %refs_5_.1, bf16[256,512]{1,0:T(8,128)(2,1)} %get-tuple-element.11.refs_6_, ...), custom_call_target="tpu_custom_call" | custom-call | tf_op jit(solution)/shard_map/pallas_call | solution.py:483
  240.9 1.9 copy.20
  (2 shorter events, 0.0 us)
Async XLA Ops:
  0.0 2.3 copy-start.6
  0.0 4.0 %copy-start = (f32[352,512]{1,0:T(8,128)S(1)}, f32[352,512]{1,0:T(8,128)}, u32[]{:S(2)}) copy-start(f32[352,512]{1,0:T(8,128)} %param.22) | copy-start | bytes 2162692
  2.3 2.5 %copy-start.1 = (f32[352,512]{1,0:T(8,128)S(1)}, f32[352,512]{1,0:T(8,128)}, u32[]{:S(2)}) copy-start(f32[352,512]{1,0:T(8,128)} %param.35) | copy-start | bytes 2162692
  4.8 0.9 copy-start.7
  4.8 1.1 copy-start.8
  6.4 1.1 copy-start.2
  6.4 1.5 copy-start.3
  7.9 1.4 copy-start.4
  7.9 1.6 copy-start.5
where the time goes:
time: 243 us
  Pallas kernels  230 us (95%)
  other arithmetic  8.5 us (3%)
  local copies, waits for them, and re-layouts  3.73 us (2%)
    pallas_call x1, Pallas kernels, fused(): pl.pallas_call(functools.partial(layer_kernel, fs_size, tp_size), out_sha...  230 us
    convert_element_type x7, other arithmetic, fused(): half_type = lambda array: array.astype(jnp.bfloat16)  6.1 us

commit v1 on v0

v1 whole, which is shorter than its diff:
```python
import functools

import jax
import jax.numpy as jnp
from jax import lax
from jax.experimental import pallas as pl
from jax.experimental.pallas import tpu as pltpu
from jax.sharding import PartitionSpec as P

SEQ_LEN = 128


EPSILON = 1e-06
DECAY_SCALE = 8.0


def normalize(values, norm_gain):
    floats = values.astype(jnp.float32)
    scaled = floats * lax.rsqrt(jnp.mean(floats * floats, axis=-1, keepdims=True) + EPSILON)
    return (scaled * norm_gain).astype(jnp.bfloat16)


def widen(residual):
    return lax.all_gather(residual, "tp", axis=1, tiled=True)


def contract(operand, stacked):
    return jnp.dot(
        operand,
        lax.all_gather(stacked.astype(jnp.bfloat16), "fs", axis=0, tiled=True),
        preferred_element_type=jnp.float32,
    )


def feed_forward(residual, norm_gain, gate_matrix, up_matrix, down_matrix):
    normed = normalize(widen(residual), norm_gain)
    products = contract(normed, jnp.concatenate((gate_matrix, up_matrix), axis=1))
    split_at = gate_matrix.shape[1]
    hidden = (jax.nn.silu(products[:, :split_at]) * products[:, split_at:]).astype(jnp.bfloat16)
    all_hidden = lax.all_gather(hidden, "tp", axis=1, tiled=True)
    return (residual.astype(jnp.float32) + 0.5 * contract(all_hidden, down_matrix)).astype(
        jnp.bfloat16
    )


def shifted(values, distance, fill):
    row = lax.broadcasted_iota(jnp.int32, values.shape, 0)
    return jnp.where(row >= distance, pltpu.roll(values, distance, 0), fill)


def mix_sequence(branch, gate_act, taps, gates, sharpness):
    width = branch.shape[1]
    count = taps.shape[0]
    convolved = branch * taps[count - 1 : count]
    for back in range(1, count):
        convolved = convolved + shifted(branch, back, 0.0) * taps[count - 1 - back : count - back]
    convolved = convolved.astype(jnp.bfloat16)
    both = jax.nn.sigmoid(jnp.dot(convolved, gates, preferred_element_type=jnp.float32))
    log_keep = -DECAY_SCALE * both[:, :width] * sharpness
    keep = jnp.exp(log_keep)
    inject = (
        jnp.sqrt(jnp.tanh(-log_keep) * (1.0 + keep * keep))
        * both[:, width:]
        * convolved.astype(jnp.float32)
    )
    distance = 1
    while distance < branch.shape[0]:
        inject = keep * shifted(inject, distance, 0.0) + inject
        keep = keep * shifted(keep, distance, 1.0)
        distance *= 2
    return (inject * jax.nn.gelu(gate_act)).astype(jnp.bfloat16)


def mix_kernel(products_ref, taps_ref, gates_ref, sharp_ref, out_ref):
    width = out_ref.shape[1]
    out_ref[...] = mix_sequence(
        products_ref[:, :width],
        products_ref[:, width:],
        taps_ref[...],
        gates_ref[...],
        sharp_ref[...],
    )


def spread_blocks(blocks):
    count, size, _ = blocks.shape
    eye = jnp.eye(count, dtype=blocks.dtype)
    wide = eye[:, None, :, None] * blocks[:, :, None, :]
    return wide.reshape(count * size, count * size).astype(jnp.bfloat16)


def recurrent_mixer(
    residual,
    norm_gain,
    branch_matrix,
    gate_matrix,
    conv_taps,
    retain_blocks,
    admit_blocks,
    decay_param,
    channel_gain,
    out_matrix,
):
    normed = normalize(widen(residual), norm_gain)
    products = contract(normed, jnp.concatenate((branch_matrix, gate_matrix), axis=1))
    width = branch_matrix.shape[1]
    rows = residual.shape[0]
    gates = jnp.concatenate((spread_blocks(retain_blocks), spread_blocks(admit_blocks)), axis=1)
    sharpness = jax.nn.softplus(-decay_param)[None, :]
    whole = lambda array: pl.BlockSpec(array.shape, lambda i: (0, 0))
    mixed_rows = pl.pallas_call(
        mix_kernel,
        grid=(rows // SEQ_LEN,),
        in_specs=[
            pl.BlockSpec((SEQ_LEN, 2 * width), lambda i: (i, 0)),
            whole(conv_taps),
            whole(gates),
            whole(sharpness),
        ],
        out_specs=pl.BlockSpec((SEQ_LEN, width), lambda i: (i, 0)),
        out_shape=jax.ShapeDtypeStruct((rows, width), jnp.bfloat16),
        cost_estimate=pl.CostEstimate(
            flops=rows * width * 1200, bytes_accessed=rows * width * 10, transcendentals=0
        ),
    )(products, conv_taps, gates, sharpness)
    all_channels = lax.all_gather(mixed_rows, "tp", axis=1, tiled=True)
    mixed_normed = normalize(all_channels, channel_gain)
    return (residual.astype(jnp.float32) + contract(mixed_normed, out_matrix)).astype(jnp.bfloat16)


TILE = SEQ_LEN
MESH = pl.DeviceIdType.MESH


def when(condition, action):
    if condition is None:
        action()
    else:
        pl.when(condition)(action)


class Exchange:
    def __init__(self):
        self.sent = []

    def send(self, source, target, send_sem, recv_sem, device, condition=None):
        copy = remote(source, target, send_sem, recv_sem, device)
        when(condition, copy.start)
        self.sent.append((copy, condition))

    def drain(self):
        for copy, condition in self.sent:
            when(condition, copy.wait_send)


def remote(source, target, send_sem, recv_sem, device):
    return pltpu.make_async_remote_copy(
        src_ref=source,
        dst_ref=target,
        send_sem=send_sem,
        recv_sem=recv_sem,
        device_id=device,
        device_id_type=MESH,
    )


def layer_kernel(fs_size, tp_size, *refs):
    (tokens, pre_gain, mix_gain, channel_gain, post_gain) = refs[:5]
    own_side = refs[5:8]
    shards = refs[8:16]
    out = refs[16]
    whole = refs[17:25]
    first, second, third, hidden_one, hidden_two, channels = refs[25:31]
    normed, gate_part, final = refs[31:34]
    side = refs[34:37]
    recv_sem, up_sem, down_sem, far_sem, pair_sem, swap_sem, keep_sem = refs[37:44]
    token_sem, token_recv, token_pass = refs[44:47]
    slot_recv, x_sem, y_sem, pass_sem = refs[47:51]
    side_sem, side_recv, out_sem, out_recv = refs[51:55]
    taps, gates, sharpness = side

    f = lax.axis_index("fs")
    t = lax.axis_index("tp")
    x = lax.rem(f, 2)
    z = f // 2
    y = t // 2
    c = lax.rem(t, 2)
    depth = fs_size // 2
    home = x == c
    away = x != c
    end = (z == 0) | (z == depth - 1)
    inner = (z > 0) & (z < depth - 1)

    mine = 2 * y + x
    beside = 2 * y + 1 - x
    behind = 2 * (1 - y) + x
    corner = 2 * (1 - y) + 1 - x
    line = 2 * z + c

    across = f + 1 - 2 * x
    other = t + 1 - 2 * c
    x_peer = {"fs": across}
    y_peer = {"tp": lax.rem(t + 2, tp_size)}
    twin = {"tp": other}
    partner = {"fs": across, "tp": other}
    skew = {"tp": lax.rem(other + 2, tp_size)}
    above = {"fs": lax.rem(f + 2, fs_size)}
    below = {"fs": lax.rem(f + fs_size - 2, fs_size)}
    above_two = {"fs": lax.rem(f + 4, fs_size)}
    below_two = {"fs": lax.rem(f + fs_size - 4, fs_size)}
    links = Exchange()

    barrier = pltpu.get_barrier_semaphore()
    greeted = [
        (x_peer, None),
        (y_peer, None),
        (twin, None),
        (partner, None),
        (skew, None),
        (above, z < depth - 1),
        (below, z > 0),
        (above_two, z < depth - 2),
        (below_two, z > 1),
    ]
    expected = 0
    for device, condition in greeted:
        when(
            condition,
            functools.partial(
                pl.semaphore_signal, barrier, inc=1, device_id=device, device_id_type=MESH
            ),
        )
        expected = expected + (1 if condition is None else condition.astype(jnp.int32))
    pl.semaphore_wait(barrier, expected)

    def block(p, owner):
        rows = shards[p].shape[0]
        return whole[p].at[pl.ds(pl.multiple_of(owner * rows, rows), rows)]

    def arrive(p, owner, condition=None):
        place = block(p, owner)
        copy = remote(place, place, pair_sem.at[p, 0], recv_sem.at[p, owner], twin)
        when(condition, copy.wait_recv)

    def swap(p):
        links.send(
            shards[p], block(p, f), swap_sem.at[p], recv_sem.at[p, f], partner, away
        )
        when(home, pltpu.make_async_copy(shards[p], block(p, f), keep_sem.at[p]).start)

    def settle(p):
        when(home, pltpu.make_async_copy(shards[p], block(p, f), keep_sem.at[p]).wait)
        arrive(p, line, away)

    def launch(p):
        place, sem = block(p, line), recv_sem.at[p, line]
        links.send(place, place, far_sem.at[p, 0], sem, above_two, z == 0)
        links.send(place, place, far_sem.at[p, 1], sem, below_two, z == depth - 1)
        links.send(place, place, up_sem.at[p, z], sem, above, z < depth - 2)
        links.send(place, place, down_sem.at[p, z], sem, below, z > 1)
        links.send(place, place, pair_sem.at[p, z], sem, twin)

    def launch_last(p):
        place, sem = block(p, line), recv_sem.at[p, line]
        up_sem_index, down_sem_index = z, z
        links.send(place, place, up_sem.at[p, up_sem_index], sem, above, z == depth - 2)
        links.send(place, place, down_sem.at[p, down_sem_index], sem, below, z == 1)

    def take(p, level, condition):
        owner = 2 * level + c
        arrive(p, owner, condition)
        place, sem = block(p, owner), recv_sem.at[p, owner]
        upward = condition & (z > 1) & (z < depth - 1) & (level < z)
        downward = condition & (z < depth - 2) & (z > 0) & (level > z)
        links.send(place, place, up_sem.at[p, level], sem, above, upward)
        links.send(place, place, down_sem.at[p, level], sem, below, downward)
        links.send(place, place, pair_sem.at[p, level], sem, twin, condition)

    def pump(p, condition):
        for distance in range(1, depth):
            for sign in (-1, 1):
                level = z + sign * distance
                exists = (level >= 0) & (level < depth)
                take(p, lax.rem(level + depth, depth), condition & exists)

    def ready(p):
        pump(p, end)
        for level in range(depth):
            arrive(p, 2 * level + 1 - c)

    def tile_rows(s):
        return pl.ds(pl.multiple_of(s * TILE, TILE), TILE)

    def tile_sends(array, index, s):
        rows = tile_rows(s)
        place, sem = array.at[mine, rows], slot_recv.at[index, mine, s]
        return (
            remote(place, place, x_sem.at[index, s], sem, x_peer),
            remote(place, place, y_sem.at[index, s], sem, y_peer),
        )

    def tile_pass(array, index, s):
        odd = lax.rem(s, 2)
        slot = behind * (1 - odd) + beside * odd
        place = array.at[slot, tile_rows(s)]
        device = {
            "fs": f + (1 - odd) * (1 - 2 * x),
            "tp": lax.rem(t + 2 * odd, tp_size),
        }
        return remote(
            place, place, pass_sem.at[index, s], slot_recv.at[index, slot, s], device
        )

    def emit(array, index, s):
        for copy in tile_sends(array, index, s):
            copy.start()

    def relay(array, index, s):
        copy = tile_pass(array, index, s)
        copy.wait_recv()
        copy.start()

    def complete(array, index, s):
        odd = lax.rem(s, 2)
        for slot in (beside * (1 - odd) + behind * odd, corner):
            place = array.at[slot, tile_rows(s)]
            remote(
                place, place, x_sem.at[index, s], slot_recv.at[index, slot, s], x_peer
            ).wait_recv()

    total_rows = tokens.shape[0]
    tiles = total_rows // TILE

    def loop(body):
        def run(s, carry):
            body(s)
            return carry

        lax.fori_loop(0, tiles, run, 0)

    def stage(index, array, work, earlier=None, before=None):
        def body(s):
            if before is not None:
                complete(before, index - 1, s)
            work(s)
            emit(array, index, s)
            if earlier is not None:
                pl.when(s == 0)(lambda: relay(earlier, index - 1, tiles - 1))
            pl.when(s > 0)(lambda: relay(array, index, s - 1))

        loop(body)

    def norm_rows(array, gain, s):
        width = array.shape[2]
        features = width * tp_size
        for piece in range(0, TILE, 64):
            rows = pl.ds(pl.multiple_of(s * TILE + piece, 64), 64)
            parts = [array[k, rows, :].astype(jnp.float32) for k in range(tp_size)]
            squares = sum(jnp.sum(part * part, axis=-1, keepdims=True) for part in parts)
            scale = lax.rsqrt(squares / features + EPSILON)
            for k, part in enumerate(parts):
                at = slice(k * width, (k + 1) * width)
                normed[rows, at] = (part * scale * gain[:, at]).astype(jnp.bfloat16)

    def dot(left, right):
        return jnp.dot(left, right, preferred_element_type=jnp.float32)

    def turned(rows, matrix):
        features = matrix.shape[1]
        width = matrix.shape[0] // fs_size
        return sum(
            lax.dot_general(
                normed[rows, k * features : (k + 1) * features],
                matrix[k * width : (k + 1) * width, :],
                (((1,), (1,)), ((), ())),
                preferred_element_type=jnp.float32,
            )
            for k in range(fs_size)
        )

    def gate_tile(matrix):
        def work(s):
            rows = tile_rows(s)
            gate_part[rows, :] = jax.nn.silu(turned(rows, matrix))

        return work

    def up_tile(matrix, hidden):
        def work(s):
            rows = tile_rows(s)
            product = gate_part[rows, :] * turned(rows, matrix)
            hidden[mine, rows, :] = product.astype(jnp.bfloat16)

        return work

    def lowered(hidden, down, residual, rows):
        width = hidden.shape[2]
        total = sum(
            dot(hidden[k, rows, :], down[k * width : (k + 1) * width, :]) for k in range(tp_size)
        )
        value = residual[mine, rows, :].astype(jnp.float32) + 0.5 * total
        return value.astype(jnp.bfloat16)

    def down_tile(s):
        rows = tile_rows(s)
        second[mine, rows, :] = lowered(hidden_one, whole[2], first, rows)

    def mix_tile(s):
        rows = tile_rows(s)
        norm_rows(second, mix_gain, s)
        width = channels.shape[2]
        products = dot(normed[rows, :], whole[3][...])
        channels[mine, rows, :] = mix_sequence(
            products[:, :width], products[:, width:], taps[...], gates[...], sharpness[...]
        )

    def out_tile(s):
        rows = tile_rows(s)
        norm_rows(channels, channel_gain, s)
        width = channels.shape[2] * tp_size
        total = dot(normed[rows, :width], whole[4][...])
        third[mine, rows, :] = (second[mine, rows, :].astype(jnp.float32) + total).astype(
            jnp.bfloat16
        )

    def out_send(s):
        rows = tile_rows(s)
        return remote(final.at[rows], out.at[rows], out_sem.at[s], out_recv.at[s], partner)

    count = len(shards)

    swap(0)
    keep_tokens = pltpu.make_async_copy(tokens, first.at[t], token_sem.at[0])
    when(home, keep_tokens.start)
    target, sem = first.at[t], token_recv.at[t]
    links.send(tokens, target, token_sem.at[1], sem, {"fs": across, "tp": 2 * y + x})
    links.send(tokens, target, token_sem.at[2], sem, {"tp": behind})
    links.send(tokens, target, token_sem.at[3], sem, twin, away)
    swap(1)
    settle(0)
    launch(0)
    launch_last(0)

    def token_arrive(slot, condition):
        place = first.at[slot]
        copy = remote(place, place, token_sem.at[1], token_recv.at[slot], y_peer)
        when(condition, copy.wait_recv)

    for k in range(2):
        slot = 2 * y + k
        token_arrive(slot, away)
        links.send(
            first.at[slot],
            first.at[slot],
            token_pass.at[k],
            token_recv.at[slot],
            y_peer,
            away,
        )
    for k, (own, target) in enumerate(zip(own_side, side)):
        links.send(own, target, side_sem.at[k], side_recv.at[k], partner, away)
        when(home, pltpu.make_async_copy(own, target, side_sem.at[k]).start)
    settle(1)
    launch(1)
    launch_last(1)
    for p in range(2, count):
        swap(p)
    when(home, keep_tokens.wait)
    token_arrive(other, home)
    token_arrive(2 * (1 - y), None)
    token_arrive(2 * (1 - y) + 1, None)
    loop(functools.partial(norm_rows, first, pre_gain))
    for p in range(2, 5):
        settle(p)
        launch(p)
    pump(0, inner)
    ready(0)
    loop(gate_tile(whole[0]))
    for p in range(5, count):
        settle(p)
        launch(p)
    pump(1, inner)
    launch_last(2)
    launch_last(3)
    ready(1)
    stage(1, hidden_one, up_tile(whole[1], hidden_one))
    pump(2, inner)
    relay(hidden_one, 1, tiles - 1)
    ready(2)
    stage(2, second, down_tile, before=hidden_one)
    pump(3, inner)
    launch_last(4)
    pump(4, inner)
    launch_last(5)
    for k, (own, target) in enumerate(zip(own_side, side)):
        when(home, pltpu.make_async_copy(own, target, side_sem.at[k]).wait)
        when(
            away, remote(own, target, side_sem.at[k], side_recv.at[k], partner).wait_recv
        )
    ready(3)
    stage(3, channels, mix_tile, earlier=second, before=second)
    pump(5, inner)
    launch_last(6)
    ready(4)
    stage(4, third, out_tile, earlier=channels, before=channels)
    relay(third, 4, tiles - 1)
    pump(6, inner)
    launch_last(7)
    ready(5)

    def post_gate_tile(s):
        complete(third, 4, s)
        norm_rows(third, post_gain, s)
        gate_tile(whole[5])(s)

    loop(post_gate_tile)
    pump(7, inner)
    ready(6)
    stage(5, hidden_two, up_tile(whole[6], hidden_two))
    relay(hidden_two, 5, tiles - 1)
    ready(7)

    def last_tile(s):
        rows = tile_rows(s)
        complete(hidden_two, 5, s)
        final[rows, :] = lowered(hidden_two, whole[7], third, rows)
        when(away, out_send(s).start)

        def keep():
            out[rows, :] = final[rows, :]

        when(home, keep)

    loop(last_tile)

    def drain_tiles(s):
        for index, array in enumerate((hidden_one, second, channels, third, hidden_two)):
            for copy in tile_sends(array, index + 1, s):
                copy.wait_send()
            tile_pass(array, index + 1, s).wait_send()
        when(away, out_send(s).wait_send)
        when(away, out_send(s).wait_recv)

    links.drain()
    loop(drain_tiles)


def fused(
    fs_size,
    tp_size,
    tokens,
    pre_gain,
    pre_gate,
    pre_up,
    pre_down,
    mix_gain,
    branch_proj,
    gate_proj,
    conv_taps,
    retain_blocks,
    admit_blocks,
    decay_param,
    channel_gain,
    out_proj,
    post_gain,
    post_gate,
    post_up,
    post_down,
):
    half_type = lambda array: array.astype(jnp.bfloat16)
    shards = [
        half_type(pre_gate.T),
        half_type(pre_up.T),
        half_type(pre_down),
        jnp.concatenate((half_type(branch_proj), half_type(gate_proj)), axis=1),
        half_type(out_proj),
        half_type(post_gate.T),
        half_type(post_up.T),
        half_type(post_down),
    ]
    gates = jnp.concatenate((spread_blocks(retain_blocks), spread_blocks(admit_blocks)), axis=1)
    sharpness = jax.nn.softplus(-decay_param)[None, :]
    rows, width = tokens.shape
    hidden = pre_gate.shape[1]
    operands = [
        tokens,
        pre_gain[None],
        mix_gain[None],
        channel_gain[None],
        post_gain[None],
        conv_taps,
        gates,
        sharpness,
        *shards,
    ]
    dma = pltpu.SemaphoreType.DMA
    count = len(shards)
    depth = fs_size // 2
    tiles = rows // TILE
    stacked = lambda columns: pltpu.VMEM((tp_size, rows, columns), jnp.bfloat16)
    return pl.pallas_call(
        functools.partial(layer_kernel, fs_size, tp_size),
        out_shape=jax.ShapeDtypeStruct(tokens.shape, tokens.dtype),
        in_specs=[pl.BlockSpec(memory_space=pltpu.VMEM)] * len(operands),
        out_specs=pl.BlockSpec(memory_space=pltpu.VMEM),
        scratch_shapes=[
            *(pltpu.VMEM((fs_size * s.shape[0], s.shape[1]), jnp.bfloat16) for s in shards),
            stacked(width),
            stacked(width),
            stacked(width),
            stacked(hidden),
            stacked(hidden),
            stacked(branch_proj.shape[1]),
            pltpu.VMEM((rows, width * tp_size), jnp.bfloat16),
            pltpu.VMEM((rows, hidden), jnp.float32),
            pltpu.VMEM((rows, width), jnp.bfloat16),
            *(pltpu.VMEM(s.shape, s.dtype) for s in (conv_taps, gates, sharpness)),
            dma((count, fs_size)),
            dma((count, depth)),
            dma((count, depth)),
            dma((count, 2)),
            dma((count, depth)),
            dma((count,)),
            dma((count,)),
            dma((4,)),
            dma((tp_size,)),
            dma((2,)),
            dma((6, tp_size, tiles)),
            dma((6, tiles)),
            dma((6, tiles)),
            dma((6, tiles)),
            dma((3,)),
            dma((3,)),
            dma((tiles,)),
            dma((tiles,)),
        ],
        compiler_params=pltpu.CompilerParams(
            collective_id=0, has_side_effects=True, vmem_limit_bytes=62 * 2**20
        ),
    )(*operands)


def fits_fused(fs_size, tp_size, arrays):
    shards = [a for i, a in enumerate(arrays) if i in (2, 3, 4, 6, 7, 13, 15, 16, 17)]
    rows_fit = all(a.shape[0] % 16 == 0 for a in shards)
    lanes_fit = all(arrays[i].shape[1] % 128 == 0 for i in (0, 6, 7))
    tiles_fit = arrays[0].shape[0] % TILE == 0 and arrays[2].shape[1] % 16 == 0
    turned_fit = all(arrays[i].shape[0] % 128 == 0 for i in (2, 3, 15, 16))
    return (
        rows_fit
        and lanes_fit
        and tiles_fit
        and turned_fit
        and fs_size % 2 == 0
        and 6 <= fs_size <= 16
        and tp_size == 4
    )


def local(
    tokens,
    pre_gain,
    pre_gate,
    pre_up,
    pre_down,
    mix_gain,
    branch_proj,
    gate_proj,
    conv_taps,
    retain_blocks,
    admit_blocks,
    decay_param,
    channel_gain,
    out_proj,
    post_gain,
    post_gate,
    post_up,
    post_down,
):
    after_pre = feed_forward(tokens, pre_gain, pre_gate, pre_up, pre_down)
    after_mix = recurrent_mixer(
        after_pre,
        mix_gain,
        branch_proj,
        gate_proj,
        conv_taps,
        retain_blocks,
        admit_blocks,
        decay_param,
        channel_gain,
        out_proj,
    )
    return feed_forward(after_mix, post_gain, post_gate, post_up, post_down)


def solution(mesh):
    placed = (
        P("fs", "tp"),
        P(),
        P("fs", "tp"),
        P("fs", "tp"),
        P("fs", "tp"),
        P(),
        P("fs", "tp"),
        P("fs", "tp"),
        P(None, "tp"),
        P("tp", None, None),
        P("tp", None, None),
        P("tp"),
        P(),
        P("fs", "tp"),
        P(),
        P("fs", "tp"),
        P("fs", "tp"),
        P("fs", "tp"),
    )
    fs_size, tp_size = mesh.shape["fs"], mesh.shape["tp"]

    def layer(*arrays):
        if fits_fused(fs_size, tp_size, arrays):
            return fused(fs_size, tp_size, *arrays)
        return local(*arrays)

    return jax.shard_map(
        layer, mesh=mesh, in_specs=placed, out_specs=P("fs", "tp"), check_vma=False
    )
```

time: 243 us -> 214 us (0.88)
  Pallas kernels: 230 us -> 201 us
    pallas_call x1, Pallas kernels: 230 us -> 201 us  [fused(): pl.pallas_call(functools.partial(layer_kernel, fs_size, tp_size), out_sha...]
where the time goes in v1:
time: 214 us
  Pallas kernels  201 us (94%)
  other arithmetic  8.5 us (4%)
  local copies, waits for them, and re-layouts  3.73 us (2%)
    pallas_call x1, Pallas kernels, fused(): pl.pallas_call(functools.partial(layer_kernel, fs_size, tp_size), out_sha...  201 us
    convert_element_type x7, other arithmetic, fused(): half_type = lambda array: array.astype(jnp.bfloat16)  6.1 us

profile of v1, /device:TPU:1, one launch (start us, length us, event | category | flops | bytes accessed | tf_op | source)
XLA Modules:
  0.0 213.8 jit_solution(17748007155442348479)
XLA Ops:
  0.0 0.0 copy-start.6
  0.0 0.0 copy-start
  0.0 1.3 compare_select_fusion
  1.3 1.0 convert_element_type.67
  2.3 0.0 copy-done.6
  2.3 0.0 copy-start.1
  2.3 1.7 convert_element_type.69.refs_12_
  4.0 0.0 copy-done
  4.0 0.8 convert_element_type.66.refs_10_
  4.8 0.0 copy-done.1
  4.8 0.0 copy-start.7
  4.8 0.0 copy-start.8
  4.8 0.8 convert_element_type.74.refs_15_
  5.6 0.1 copy-done.7
  5.7 0.2 copy-done.8
  5.9 0.3 multiply_convert_fusion.1
  6.2 0.2 convert_element_type.59
  6.4 0.0 copy-start.2
  6.4 0.0 copy-start.3
  6.4 0.2 convert_element_type.61
  6.6 0.8 pad_maximum_fusion
  7.5 0.0 copy-done.2
  7.5 0.4 copy-done.3
  7.9 0.0 copy-start.4
  7.9 0.0 copy-start.5
  7.9 0.9 convert_bitcast_fusion.2
  8.8 0.4 copy-done.4
  9.3 0.2 copy-done.5
  9.5 0.9 convert_bitcast_fusion
  10.4 201.5 %shard_map.172 = bf16[512,512]{1,0:T(8,128)(2,1)} custom-call(bf16[512,512]{1,0:T(8,128)(2,1)} %refs_0_.1, f32[1,2048]{1,0:T(1,128)} %bitcast.13, f32[1,2048]{1,0:T(1,128)} %bitcast.14, f32[1,1024]{1,0:T(1,128)} %bitcast.17, f32[1,2048]{1,0:T(1,128)} %bitcast.15, f32[4,256]{1,0:T(4,128)} %refs_5_.1, bf16[256,512]{1,0:T(8,128)(2,1)} %get-tuple-element.11.refs_6_, ...), custom_call_target="tpu_custom_call" | custom-call | tf_op jit(solution)/shard_map/pallas_call | solution.py:601
  211.9 1.9 copy.20
  (2 shorter events, 0.0 us)
Async XLA Ops:
  0.0 2.3 %copy-start.6 = (f32[256,256]{1,0:T(8,128)S(1)}, f32[256,256]{1,0:T(8,128)}, u32[]{:S(2)}) copy-start(f32[256,256]{1,0:T(8,128)} %param.25) | copy-start | bytes 786436
  0.0 4.0 %copy-start = (f32[352,512]{1,0:T(8,128)S(1)}, f32[352,512]{1,0:T(8,128)}, u32[]{:S(2)}) copy-start(f32[352,512]{1,0:T(8,128)} %param.22) | copy-start | bytes 2162692
  2.3 2.5 %copy-start.1 = (f32[352,512]{1,0:T(8,128)S(1)}, f32[352,512]{1,0:T(8,128)}, u32[]{:S(2)}) copy-start(f32[352,512]{1,0:T(8,128)} %param.35) | copy-start | bytes 2162692
  4.8 0.9 copy-start.7
  4.8 1.1 copy-start.8
  6.4 1.1 copy-start.2
  6.4 1.5 copy-start.3
  7.9 1.4 copy-start.4
  7.9 1.6 copy-start.5

commit v2 on v1

--- a/solution.py
+++ b/solution.py
@@ -129,6 +129,7 @@
 
 
 TILE = SEQ_LEN
+OUT_SPACE = pltpu.VMEM
 MESH = pl.DeviceIdType.MESH
 
 
@@ -164,20 +165,29 @@
     )
 
 
+def softplus(values):
+    return jnp.maximum(values, 0.0) + jnp.log1p(jnp.exp(-jnp.abs(values)))
+
+
 def layer_kernel(fs_size, tp_size, *refs):
     (tokens, pre_gain, mix_gain, channel_gain, post_gain) = refs[:5]
-    own_side = refs[5:8]
+    own_side = refs[5:9]
+    matrices = refs[9:18]
+    out = refs[18]
+    refs = refs[19:]
+    whole = refs[:8]
     shards = refs[8:16]
-    out = refs[16]
-    whole = refs[17:25]
-    first, second, third, hidden_one, hidden_two, channels = refs[25:31]
-    normed, gate_part, final = refs[31:34]
-    side = refs[34:37]
-    recv_sem, up_sem, down_sem, far_sem, pair_sem, swap_sem, keep_sem = refs[37:44]
-    token_sem, token_recv, token_pass = refs[44:47]
-    slot_recv, x_sem, y_sem, pass_sem = refs[47:51]
-    side_sem, side_recv, out_sem, out_recv = refs[51:55]
-    taps, gates, sharpness = side
+    raw = refs[16:25]
+    first, second, third, channels = refs[25:29]
+    hidden_one, hidden_two = refs[29:31], refs[31:33]
+    normed, final, gates = refs[33:36]
+    refs = refs[1:]
+    side = refs[35:39]
+    recv_sem, up_sem, down_sem, pair_sem, swap_sem, keep_sem, raw_sem = refs[39:46]
+    token_sem, token_recv, token_pass = refs[46:49]
+    slot_recv, x_sem, y_sem, pass_sem = refs[49:53]
+    side_sem, side_recv, out_sem, out_recv = refs[53:57]
+    taps, retain, admit, decay = side
 
     f = lax.axis_index("fs")
     t = lax.axis_index("tp")
@@ -206,9 +216,40 @@
     skew = {"tp": lax.rem(other + 2, tp_size)}
     above = {"fs": lax.rem(f + 2, fs_size)}
     below = {"fs": lax.rem(f + fs_size - 2, fs_size)}
-    above_two = {"fs": lax.rem(f + 4, fs_size)}
-    below_two = {"fs": lax.rem(f + fs_size - 4, fs_size)}
     links = Exchange()
+
+    def load(m):
+        return pltpu.make_async_copy(matrices[m], raw[m], raw_sem.at[m])
+
+    for m in range(len(matrices)):
+        load(m).start()
+
+    def turn(source, halves, at):
+        width = source.shape[1]
+        half = width // 2
+        for start in range(0, width, 128):
+            stop = min(start + 128, width)
+            piece = source[:, start:stop].T.astype(jnp.bfloat16)
+            for k, target in enumerate(halves):
+                low, high = max(start, k * half), min(stop, (k + 1) * half)
+                if low < high:
+                    to = at + low - k * half
+                    target[to : to + high - low, :] = piece[low - start : high - start, :]
+
+    def copy_in(source, target, at):
+        target[:, at : at + source.shape[1]] = source[...].astype(jnp.bfloat16)
+
+    def convert(p):
+        parts = {0: (0, 1), 2: (2,), 3: (3, 4), 4: (5,), 5: (6, 7), 7: (8,)}.get(p, ())
+        at = 0
+        for m in parts:
+            load(m).wait()
+            if p in (0, 5):
+                turn(raw[m], shards[p : p + 2], at)
+                at += raw[m].shape[1] // 2
+            else:
+                copy_in(raw[m], shards[p], at)
+                at += raw[m].shape[1]
 
     barrier = pltpu.get_barrier_semaphore()
     greeted = [
@@ -219,8 +260,6 @@
         (skew, None),
         (above, z < depth - 1),
         (below, z > 0),
-        (above_two, z < depth - 2),
-        (below_two, z > 1),
     ]
     expected = 0
     for device, condition in greeted:
@@ -231,6 +270,7 @@
             ),
         )
         expected = expected + (1 if condition is None else condition.astype(jnp.int32))
+    convert(0)
     pl.semaphore_wait(barrier, expected)
 
     def block(p, owner):
@@ -248,30 +288,24 @@
         )
         when(home, pltpu.make_async_copy(shards[p], block(p, f), keep_sem.at[p]).start)
 
-    def settle(p):
-        when(home, pltpu.make_async_copy(shards[p], block(p, f), keep_sem.at[p]).wait)
-        arrive(p, line, away)
-
-    def launch(p):
+    def settle(p, who=None):
+        if who is None or who == "home":
+            when(home, pltpu.make_async_copy(shards[p], block(p, f), keep_sem.at[p]).wait)
+        if who is None or who == "away":
+            arrive(p, line, away)
+
+    def launch(p, who):
         place, sem = block(p, line), recv_sem.at[p, line]
-        links.send(place, place, far_sem.at[p, 0], sem, above_two, z == 0)
-        links.send(place, place, far_sem.at[p, 1], sem, below_two, z == depth - 1)
-        links.send(place, place, up_sem.at[p, z], sem, above, z < depth - 2)
-        links.send(place, place, down_sem.at[p, z], sem, below, z > 1)
-        links.send(place, place, pair_sem.at[p, z], sem, twin)
-
-    def launch_last(p):
-        place, sem = block(p, line), recv_sem.at[p, line]
-        up_sem_index, down_sem_index = z, z
-        links.send(place, place, up_sem.at[p, up_sem_index], sem, above, z == depth - 2)
-        links.send(place, place, down_sem.at[p, down_sem_index], sem, below, z == 1)
+        links.send(place, place, up_sem.at[p, z], sem, above, who & (z < depth - 1))
+        links.send(place, place, down_sem.at[p, z], sem, below, who & (z > 0))
+        links.send(place, place, pair_sem.at[p, z], sem, twin, who)
 
     def take(p, level, condition):
         owner = 2 * level + c
         arrive(p, owner, condition)
         place, sem = block(p, owner), recv_sem.at[p, owner]
-        upward = condition & (z > 1) & (z < depth - 1) & (level < z)
-        downward = condition & (z < depth - 2) & (z > 0) & (level > z)
+        upward = condition & (z < depth - 1) & (level < z)
+        downward = condition & (z > 0) & (level > z)
         links.send(place, place, up_sem.at[p, level], sem, above, upward)
         links.send(place, place, down_sem.at[p, level], sem, below, downward)
         links.send(place, place, pair_sem.at[p, level], sem, twin, condition)
@@ -286,7 +320,10 @@
     def ready(p):
         pump(p, end)
         for level in range(depth):
-            arrive(p, 2 * level + 1 - c)
+            if p == 0:
+                arrive(p, 2 * level + 1 - c, away | (z != level))
+            else:
+                arrive(p, 2 * level + 1 - c)
 
     def tile_rows(s):
         return pl.ds(pl.multiple_of(s * TILE, TILE), TILE)
@@ -338,14 +375,15 @@
 
         lax.fori_loop(0, tiles, run, 0)
 
-    def stage(index, array, work, earlier=None, before=None):
+    def stage(index, array, work, earlier=None, before=()):
         def body(s):
-            if before is not None:
-                complete(before, index - 1, s)
+            for k, ready_array in before:
+                complete(ready_array, k, s)
             work(s)
             emit(array, index, s)
             if earlier is not None:
-                pl.when(s == 0)(lambda: relay(earlier, index - 1, tiles - 1))
+                k, ready_array = earlier
+                pl.when(s == 0)(lambda: relay(ready_array, k, tiles - 1))
             pl.when(s > 0)(lambda: relay(array, index, s - 1))
 
         loop(body)
@@ -365,38 +403,37 @@
     def dot(left, right):
         return jnp.dot(left, right, preferred_element_type=jnp.float32)
 
-    def turned(rows, matrix):
+    def turned(rows, matrix, part):
         features = matrix.shape[1]
         width = matrix.shape[0] // fs_size
+        half = width // 2
         return sum(
             lax.dot_general(
                 normed[rows, k * features : (k + 1) * features],
-                matrix[k * width : (k + 1) * width, :],
+                matrix[k * width + part * half : k * width + (part + 1) * half, :],
                 (((1,), (1,)), ((), ())),
                 preferred_element_type=jnp.float32,
             )
             for k in range(fs_size)
         )
 
-    def gate_tile(matrix):
+    def hidden_tile(matrix, hidden):
         def work(s):
             rows = tile_rows(s)
-            gate_part[rows, :] = jax.nn.silu(turned(rows, matrix))
+            product = jax.nn.silu(turned(rows, matrix, 0)) * turned(rows, matrix, 1)
+            hidden[mine, rows, :] = product.astype(jnp.bfloat16)
 
         return work
 
-    def up_tile(matrix, hidden):
-        def work(s):
-            rows = tile_rows(s)
-            product = gate_part[rows, :] * turned(rows, matrix)
-            hidden[mine, rows, :] = product.astype(jnp.bfloat16)
-
-        return work
-
-    def lowered(hidden, down, residual, rows):
-        width = hidden.shape[2]
+    def lowered(halves, down, residual, rows):
+        half = halves[0].shape[2]
         total = sum(
-            dot(hidden[k, rows, :], down[k * width : (k + 1) * width, :]) for k in range(tp_size)
+            dot(
+                hidden[k, rows, :],
+                down[(2 * k + part) * half : (2 * k + part + 1) * half, :],
+            )
+            for k in range(tp_size)
+            for part, hidden in enumerate(halves)
         )
         value = residual[mine, rows, :].astype(jnp.float32) + 0.5 * total
         return value.astype(jnp.bfloat16)
@@ -411,7 +448,7 @@
         width = channels.shape[2]
         products = dot(normed[rows, :], whole[3][...])
         channels[mine, rows, :] = mix_sequence(
-            products[:, :width], products[:, width:], taps[...], gates[...], sharpness[...]
+            products[:, :width], products[:, width:], taps[...], gates[...], softplus(-decay[...])
         )
 
     def out_tile(s):
@@ -427,25 +464,68 @@
         rows = tile_rows(s)
         return remote(final.at[rows], out.at[rows], out_sem.at[s], out_recv.at[s], partner)
 
+    def out_keep(s):
+        rows = tile_rows(s)
+        return pltpu.make_async_copy(final.at[rows], out.at[rows], out_sem.at[s])
+
+    def spread(blocks, at):
+        size = blocks.shape[1]
+        for k in range(blocks.shape[0]):
+            place = slice(k * size, (k + 1) * size)
+            gates[place, at + k * size : at + (k + 1) * size] = blocks[k].astype(jnp.bfloat16)
+
     count = len(shards)
+    gates[...] = jnp.zeros_like(gates)
+
+    def token_arrive(slot, condition):
+        place = first.at[slot]
+        copy = remote(place, place, token_sem.at[1], token_recv.at[slot], y_peer)
+        when(condition, copy.wait_recv)
+
+    def token_cross(who):
+        links.send(
+            tokens,
+            first.at[t],
+            token_sem.at[1],
+            token_recv.at[t],
+            {"fs": across, "tp": 2 * y + x},
+            who,
+        )
+
+    def side_copies():
+        for k, (own, target) in enumerate(zip(own_side, side)):
+            yield (
+                remote(own, target, side_sem.at[k], side_recv.at[k], partner),
+                pltpu.make_async_copy(own, target, side_sem.at[k]),
+            )
 
     swap(0)
     keep_tokens = pltpu.make_async_copy(tokens, first.at[t], token_sem.at[0])
     when(home, keep_tokens.start)
     target, sem = first.at[t], token_recv.at[t]
-    links.send(tokens, target, token_sem.at[1], sem, {"fs": across, "tp": 2 * y + x})
     links.send(tokens, target, token_sem.at[2], sem, {"tp": behind})
     links.send(tokens, target, token_sem.at[3], sem, twin, away)
+    settle(0, "home")
+    launch(0, home)
+    convert(1)
     swap(1)
-    settle(0)
-    launch(0)
-    launch_last(0)
-
-    def token_arrive(slot, condition):
-        place = first.at[slot]
-        copy = remote(place, place, token_sem.at[1], token_recv.at[slot], y_peer)
-        when(condition, copy.wait_recv)
-
+    token_cross(away)
+    settle(1, "home")
+    launch(1, home)
+    arrive(0, 2 * z + 1 - c, home)
+    token_cross(home)
+    settle(0, "away")
+    launch(0, away)
+    for p in range(2, count):
+        convert(p)
+        swap(p)
+    for p in range(2, count):
+        settle(p, "home")
+        launch(p, home & end)
+    pump(0, inner & home)
+    settle(1, "away")
+    launch(1, away)
+    pump(0, inner & away)
     for k in range(2):
         slot = 2 * y + k
         token_arrive(slot, away)
@@ -457,89 +537,83 @@
             y_peer,
             away,
         )
-    for k, (own, target) in enumerate(zip(own_side, side)):
-        links.send(own, target, side_sem.at[k], side_recv.at[k], partner, away)
-        when(home, pltpu.make_async_copy(own, target, side_sem.at[k]).start)
-    settle(1)
-    launch(1)
-    launch_last(1)
-    for p in range(2, count):
-        swap(p)
+    for away_copy, home_copy in side_copies():
+        when(away, away_copy.start)
+        when(home, home_copy.start)
     when(home, keep_tokens.wait)
     token_arrive(other, home)
-    token_arrive(2 * (1 - y), None)
-    token_arrive(2 * (1 - y) + 1, None)
+    token_arrive(2 * (1 - y), home)
+    token_arrive(2 * (1 - y) + 1, home)
+    pump(1, inner)
+    for p in range(2, 4):
+        settle(p, "away")
+        launch(p, inner | away)
+    token_arrive(2 * (1 - y), away)
+    token_arrive(2 * (1 - y) + 1, away)
     loop(functools.partial(norm_rows, first, pre_gain))
-    for p in range(2, 5):
-        settle(p)
-        launch(p)
-    pump(0, inner)
     ready(0)
-    loop(gate_tile(whole[0]))
-    for p in range(5, count):
-        settle(p)
-        launch(p)
-    pump(1, inner)
-    launch_last(2)
-    launch_last(3)
+    stage(1, hidden_one[0], hidden_tile(whole[0], hidden_one[0]))
+    for p in range(4, count):
+        settle(p, "away")
+        launch(p, away & end)
+    pump(2, inner)
+    launch(4, inner)
+    relay(hidden_one[0], 1, tiles - 1)
     ready(1)
-    stage(1, hidden_one, up_tile(whole[1], hidden_one))
-    pump(2, inner)
-    relay(hidden_one, 1, tiles - 1)
+    stage(2, hidden_one[1], hidden_tile(whole[1], hidden_one[1]))
+    pump(3, inner)
+    launch(5, inner)
+    relay(hidden_one[1], 2, tiles - 1)
+    for away_copy, home_copy in side_copies():
+        when(away, away_copy.wait)
+        when(home, home_copy.wait)
+    spread(retain, 0)
+    spread(admit, gates.shape[0])
     ready(2)
-    stage(2, second, down_tile, before=hidden_one)
-    pump(3, inner)
-    launch_last(4)
+    stage(3, second, down_tile, before=((1, hidden_one[0]), (2, hidden_one[1])))
     pump(4, inner)
-    launch_last(5)
-    for k, (own, target) in enumerate(zip(own_side, side)):
-        when(home, pltpu.make_async_copy(own, target, side_sem.at[k]).wait)
-        when(
-            away, remote(own, target, side_sem.at[k], side_recv.at[k], partner).wait_recv
-        )
+    pump(5, inner)
+    launch(6, inner)
     ready(3)
-    stage(3, channels, mix_tile, earlier=second, before=second)
-    pump(5, inner)
-    launch_last(6)
+    stage(4, channels, mix_tile, earlier=(3, second), before=((3, second),))
+    pump(6, inner)
+    launch(7, inner)
     ready(4)
-    stage(4, third, out_tile, earlier=channels, before=channels)
-    relay(third, 4, tiles - 1)
-    pump(6, inner)
-    launch_last(7)
+    stage(5, third, out_tile, earlier=(4, channels), before=((4, channels),))
+    pump(7, inner)
+    relay(third, 5, tiles - 1)
     ready(5)
-
-    def post_gate_tile(s):
-        complete(third, 4, s)
+    post_tile = hidden_tile(whole[5], hidden_two[0])
+
+    def post_norm_tile(s):
         norm_rows(third, post_gain, s)
-        gate_tile(whole[5])(s)
-
-    loop(post_gate_tile)
-    pump(7, inner)
+        post_tile(s)
+
+    stage(6, hidden_two[0], post_norm_tile, before=((5, third),))
+    relay(hidden_two[0], 6, tiles - 1)
     ready(6)
-    stage(5, hidden_two, up_tile(whole[6], hidden_two))
-    relay(hidden_two, 5, tiles - 1)
+    stage(7, hidden_two[1], hidden_tile(whole[6], hidden_two[1]))
+    relay(hidden_two[1], 7, tiles - 1)
     ready(7)
 
     def last_tile(s):
         rows = tile_rows(s)
-        complete(hidden_two, 5, s)
+        complete(hidden_two[0], 6, s)
+        complete(hidden_two[1], 7, s)
         final[rows, :] = lowered(hidden_two, whole[7], third, rows)
         when(away, out_send(s).start)
-
-        def keep():
-            out[rows, :] = final[rows, :]
-
-        when(home, keep)
+        when(home, out_keep(s).start)
 
     loop(last_tile)
+    gathered = (*hidden_one, second, channels, third, *hidden_two)
 
     def drain_tiles(s):
-        for index, array in enumerate((hidden_one, second, channels, third, hidden_two)):
+        for index, array in enumerate(gathered):
             for copy in tile_sends(array, index + 1, s):
                 copy.wait_send()
             tile_pass(array, index + 1, s).wait_send()
-        when(away, out_send(s).wait_send)
-        when(away, out_send(s).wait_recv)
+        when(away, out_send(s).wait)
+        when(home, out_keep(s).wait)
 
     links.drain()
     loop(drain_tiles)
@@ -567,31 +641,39 @@
     post_up,
     post_down,
 ):
-    half_type = lambda array: array.astype(jnp.bfloat16)
+    matrices = [
+        pre_gate,
+        pre_up,
+        pre_down,
+        branch_proj,
+        gate_proj,
+        out_proj,
+        post_gate,
+        post_up,
+        post_down,
+    ]
     shards = [
-        half_type(pre_gate.T),
-        half_type(pre_up.T),
-        half_type(pre_down),
-        jnp.concatenate((half_type(branch_proj), half_type(gate_proj)), axis=1),
-        half_type(out_proj),
-        half_type(post_gate.T),
-        half_type(post_up.T),
-        half_type(post_down),
+        pre_gate.shape[::-1],
+        pre_gate.shape[::-1],
+        pre_down.shape,
+        (branch_proj.shape[0], branch_proj.shape[1] + gate_proj.shape[1]),
+        out_proj.shape,
+        post_gate.shape[::-1],
+        post_gate.shape[::-1],
+        post_down.shape,
     ]
-    gates = jnp.concatenate((spread_blocks(retain_blocks), spread_blocks(admit_blocks)), axis=1)
-    sharpness = jax.nn.softplus(-decay_param)[None, :]
     rows, width = tokens.shape
     hidden = pre_gate.shape[1]
+    channels = branch_proj.shape[1]
+    side = [conv_taps, retain_blocks, admit_blocks, decay_param[None]]
     operands = [
         tokens,
         pre_gain[None],
         mix_gain[None],
         channel_gain[None],
         post_gain[None],
-        conv_taps,
-        gates,
-        sharpness,
-        *shards,
+        *side,
+        *matrices,
     ]
     dma = pltpu.SemaphoreType.DMA
     count = len(shards)
@@ -601,36 +683,41 @@
     return pl.pallas_call(
         functools.partial(layer_kernel, fs_size, tp_size),
         out_shape=jax.ShapeDtypeStruct(tokens.shape, tokens.dtype),
-        in_specs=[pl.BlockSpec(memory_space=pltpu.VMEM)] * len(operands),
-        out_specs=pl.BlockSpec(memory_space=pltpu.VMEM),
+        in_specs=[pl.BlockSpec(memory_space=pltpu.VMEM)] * (5 + len(side))
+        + [pl.BlockSpec(memory_space=pl.ANY)] * len(matrices),
+        out_specs=pl.BlockSpec(memory_space=OUT_SPACE),
         scratch_shapes=[
-            *(pltpu.VMEM((fs_size * s.shape[0], s.shape[1]), jnp.bfloat16) for s in shards),
+            *(pltpu.VMEM((fs_size * s[0], s[1]), jnp.bfloat16) for s in shards),
+            *(pltpu.VMEM(s, jnp.bfloat16) for s in shards),
+            *(pltpu.VMEM(m.shape, m.dtype) for m in matrices),
             stacked(width),
             stacked(width),
             stacked(width),
-            stacked(hidden),
-            stacked(hidden),
-            stacked(branch_proj.shape[1]),
+            stacked(channels),
+            stacked(hidden // 2),
+            stacked(hidden // 2),
+            stacked(hidden // 2),
+            stacked(hidden // 2),
             pltpu.VMEM((rows, width * tp_size), jnp.bfloat16),
-            pltpu.VMEM((rows, hidden), jnp.float32),
             pltpu.VMEM((rows, width), jnp.bfloat16),
-            *(pltpu.VMEM(s.shape, s.dtype) for s in (conv_taps, gates, sharpness)),
+            pltpu.VMEM((channels, 2 * channels), jnp.bfloat16),
+            *(pltpu.VMEM(s.shape, s.dtype) for s in side),
             dma((count, fs_size)),
             dma((count, depth)),
             dma((count, depth)),
-            dma((count, 2)),
             dma((count, depth)),
             dma((count,)),
             dma((count,)),
+            dma((len(matrices),)),
             dma((4,)),
             dma((tp_size,)),
             dma((2,)),
-            dma((6, tp_size, tiles)),
-            dma((6, tiles)),
-            dma((6, tiles)),
-            dma((6, tiles)),
-            dma((3,)),
-            dma((3,)),
+            dma((8, tp_size, tiles)),
+            dma((8, tiles)),
+            dma((8, tiles)),
+            dma((8, tiles)),
+            dma((len(side),)),
+            dma((len(side),)),
             dma((tiles,)),
             dma((tiles,)),
         ],
@@ -644,7 +731,7 @@
     shards = [a for i, a in enumerate(arrays) if i in (2, 3, 4, 6, 7, 13, 15, 16, 17)]
     rows_fit = all(a.shape[0] % 16 == 0 for a in shards)
     lanes_fit = all(arrays[i].shape[1] % 128 == 0 for i in (0, 6, 7))
-    tiles_fit = arrays[0].shape[0] % TILE == 0 and arrays[2].shape[1] % 16 == 0
+    tiles_fit = arrays[0].shape[0] % TILE == 0 and arrays[2].shape[1] % 32 == 0
     turned_fit = all(arrays[i].shape[0] % 128 == 0 for i in (2, 3, 15, 16))
     return (
         rows_fit

time: 214 us -> 197 us (0.921)
  the two profiles are of different devices: /device:TPU:1 before, /device:TPU:13 now
where the time goes in v2:
time: 197 us
  Pallas kernels  189 us (96%)
  local copies, waits for them, and re-layouts  7.72 us (4%)
    pallas_call x1, Pallas kernels, fused(): pl.pallas_call(functools.partial(layer_kernel, fs_size, tp_size), out_sha...  189 us
    unnamed x11, local copies, waits for them, and re-layouts  7.72 us

profile of v2, /device:TPU:13, one launch (start us, length us, event | category | flops | bytes accessed | tf_op | source)
XLA Modules:
  0.0 196.5 jit_solution(15275465307450808942)
XLA Ops:
  0.0 0.0 copy-start
  0.0 2.3 %copy.19.refs_9_ = f32[256,704]{1,0:T(8,128)} copy(f32[256,704]{0,1:T(8,128)} %param.20) | data formatting | bytes 1441792 | tf_op args[2]
  2.3 0.0 copy-done
  2.3 0.0 copy-start.1
  2.3 1.2 copy.20.refs_10_
  3.5 0.0 copy-done.1
  3.5 0.0 copy-start.2
  3.5 1.2 copy.21.refs_15_
  4.7 0.0 copy-done.2
  4.7 1.2 copy.22.refs_16_
  5.9 188.8 %shard_map.172 = bf16[512,512]{1,0:T(8,128)(2,1)} custom-call(bf16[512,512]{1,0:T(8,128)(2,1)} %refs_0_.1, f32[1,2048]{1,0:T(1,128)} %bitcast.5, f32[1,2048]{1,0:T(1,128)} %bitcast.6, f32[1,1024]{1,0:T(1,128)} %bitcast.8, f32[1,2048]{1,0:T(1,128)} %bitcast.7, f32[4,256]{1,0:T(4,128)} %refs_5_.1, f32[4,64,64]{2,1,0:T(8,128)} %refs_6_.1, ...), custom_call_target="tpu_custom_call" | custom-call | tf_op jit(solution)/shard_map/pallas_call | solution.py:683
  194.7 1.9 copy.24
Async XLA Ops:
  0.0 2.3 %copy-start = (f32[256,704]{0,1:T(8,128)S(1)}, f32[256,704]{0,1:T(8,128)}, u32[]{:S(2)}) copy-start(f32[256,704]{0,1:T(8,128)} %param.21) | copy-start | bytes 2162692
  2.3 1.2 copy-start.1
  3.5 1.2 copy-start.2

commit v3 on v2

--- a/solution.py
+++ b/solution.py
@@ -129,7 +129,7 @@
 
 
 TILE = SEQ_LEN
-OUT_SPACE = pltpu.VMEM
+TAKEN = 3
 MESH = pl.DeviceIdType.MESH
 
 
@@ -175,18 +175,19 @@
     matrices = refs[9:18]
     out = refs[18]
     refs = refs[19:]
-    whole = refs[:8]
-    shards = refs[8:16]
-    raw = refs[16:25]
+    whole = refs[:9]
+    shards = refs[9:18]
+    raw = refs[18:27]
+    refs = refs[2:]
     first, second, third, channels = refs[25:29]
     hidden_one, hidden_two = refs[29:31], refs[31:33]
     normed, final, gates = refs[33:36]
     refs = refs[1:]
     side = refs[35:39]
-    recv_sem, up_sem, down_sem, pair_sem, swap_sem, keep_sem, raw_sem = refs[39:46]
+    recv_sem, twin_sem, pace_sem, own_sem, take_sem, swap_sem, raw_sem = refs[39:46]
     token_sem, token_recv, token_pass = refs[46:49]
-    slot_recv, x_sem, y_sem, pass_sem = refs[49:53]
-    side_sem, side_recv, out_sem, out_recv = refs[53:57]
+    slot_recv, slot_sem = refs[49:51]
+    side_sem, side_recv, out_sem, out_recv = refs[51:55]
     taps, retain, admit, decay = side
 
     f = lax.axis_index("fs")
@@ -224,31 +225,24 @@
     for m in range(len(matrices)):
         load(m).start()
 
-    def turn(source, halves, at):
-        width = source.shape[1]
-        half = width // 2
-        for start in range(0, width, 128):
-            stop = min(start + 128, width)
-            piece = source[:, start:stop].T.astype(jnp.bfloat16)
-            for k, target in enumerate(halves):
-                low, high = max(start, k * half), min(stop, (k + 1) * half)
-                if low < high:
-                    to = at + low - k * half
-                    target[to : to + high - low, :] = piece[low - start : high - start, :]
-
-    def copy_in(source, target, at):
-        target[:, at : at + source.shape[1]] = source[...].astype(jnp.bfloat16)
-
     def convert(p):
         parts = {0: (0, 1), 2: (2,), 3: (3, 4), 4: (5,), 5: (6, 7), 7: (8,)}.get(p, ())
         at = 0
         for m in parts:
             load(m).wait()
             if p in (0, 5):
-                turn(raw[m], shards[p : p + 2], at)
-                at += raw[m].shape[1] // 2
+                half = raw[m].shape[0] // 2
+                for k in range(2):
+                    shards[p + k][at : at + half, :] = raw[m][
+                        k * half : (k + 1) * half, :
+                    ].astype(jnp.bfloat16)
+                at += half
+            elif p == 7:
+                cut = shards[7].shape[1]
+                shards[7][...] = raw[m][:, :cut].astype(jnp.bfloat16)
+                shards[8][...] = raw[m][:, cut:].astype(jnp.bfloat16)
             else:
-                copy_in(raw[m], shards[p], at)
+                shards[p][:, at : at + raw[m].shape[1]] = raw[m][...].astype(jnp.bfloat16)
                 at += raw[m].shape[1]
 
     barrier = pltpu.get_barrier_semaphore()
@@ -277,66 +271,84 @@
         rows = shards[p].shape[0]
         return whole[p].at[pl.ds(pl.multiple_of(owner * rows, rows), rows)]
 
-    def arrive(p, owner, condition=None):
-        place = block(p, owner)
-        copy = remote(place, place, pair_sem.at[p, 0], recv_sem.at[p, owner], twin)
+    def arrive(p, level, condition=None):
+        place = block(p, 2 * level + c)
+        copy = remote(place, place, own_sem.at[p, 0], recv_sem.at[p, level], twin)
         when(condition, copy.wait_recv)
 
+    def arrive_twin(p, blocks, sem, condition=None):
+        place = whole[p].at[pl.ds(0, blocks * shards[p].shape[0])]
+        copy = remote(place, place, own_sem.at[p, 0], sem, twin)
+        when(condition, copy.wait_recv)
+
     def swap(p):
-        links.send(
-            shards[p], block(p, f), swap_sem.at[p], recv_sem.at[p, f], partner, away
-        )
-        when(home, pltpu.make_async_copy(shards[p], block(p, f), keep_sem.at[p]).start)
+        links.send(shards[p], block(p, f), swap_sem.at[p], recv_sem.at[p, z], partner, away)
+        when(home, pltpu.make_async_copy(shards[p], block(p, f), swap_sem.at[p]).start)
 
     def settle(p, who=None):
         if who is None or who == "home":
-            when(home, pltpu.make_async_copy(shards[p], block(p, f), keep_sem.at[p]).wait)
+            when(home, pltpu.make_async_copy(shards[p], block(p, f), swap_sem.at[p]).wait)
         if who is None or who == "away":
-            arrive(p, line, away)
+            arrive(p, z, away)
 
     def launch(p, who):
-        place, sem = block(p, line), recv_sem.at[p, line]
-        links.send(place, place, up_sem.at[p, z], sem, above, who & (z < depth - 1))
-        links.send(place, place, down_sem.at[p, z], sem, below, who & (z > 0))
-        links.send(place, place, pair_sem.at[p, z], sem, twin, who)
-
-    def take(p, level, condition):
-        owner = 2 * level + c
-        arrive(p, owner, condition)
-        place, sem = block(p, owner), recv_sem.at[p, owner]
-        upward = condition & (z < depth - 1) & (level < z)
-        downward = condition & (z > 0) & (level > z)
-        links.send(place, place, up_sem.at[p, level], sem, above, upward)
-        links.send(place, place, down_sem.at[p, level], sem, below, downward)
-        links.send(place, place, pair_sem.at[p, level], sem, twin, condition)
+        place, sem = block(p, line), recv_sem.at[p, z]
+        links.send(place, place, own_sem.at[p, 1], sem, above, who & (z < depth - 2))
+        links.send(place, place, own_sem.at[p, 2], sem, below, who & (z > 1))
+        sem = pace_sem if p == 0 else twin_sem.at[p]
+        links.send(place, place, own_sem.at[p, 0], sem, twin, who)
+
+    def launch_last(p, who):
+        place, sem = block(p, line), recv_sem.at[p, z]
+        links.send(place, place, own_sem.at[p, 1], sem, above, who & (z == depth - 2))
+        links.send(place, place, own_sem.at[p, 2], sem, below, who & (z == 1))
+
+    taken = {}
+
+    def take(p, key, level, condition):
+        for copy, earlier in taken.get((p - TAKEN, key), ()):
+            when(condition & earlier, copy.wait_send)
+        arrive(p, level, condition)
+        place = block(p, 2 * level + c)
+        sends = (
+            (recv_sem.at[p, level], above, condition & (z < depth - 1) & (level < z)),
+            (recv_sem.at[p, level], below, condition & (z > 0) & (level > z)),
+            (twin_sem.at[p], twin, condition),
+        )
+        for k, (sem, device, who) in enumerate(sends):
+            copy = remote(place, place, take_sem.at[p % TAKEN, k, level], sem, device)
+            when(who, copy.start)
+            taken.setdefault((p, key), []).append((copy, who))
 
     def pump(p, condition):
         for distance in range(1, depth):
             for sign in (-1, 1):
                 level = z + sign * distance
                 exists = (level >= 0) & (level < depth)
-                take(p, lax.rem(level + depth, depth), condition & exists)
+                take(p, sign * distance, lax.rem(level + depth, depth), condition & exists)
 
     def ready(p):
         pump(p, end)
-        for level in range(depth):
-            if p == 0:
-                arrive(p, 2 * level + 1 - c, away | (z != level))
-            else:
-                arrive(p, 2 * level + 1 - c)
+        if p == 0:
+            arrive_twin(p, 1, pace_sem, away)
+            arrive_twin(p, depth - 1, twin_sem.at[p])
+        else:
+            arrive_twin(p, depth, twin_sem.at[p])
 
     def tile_rows(s):
         return pl.ds(pl.multiple_of(s * TILE, TILE), TILE)
 
     def tile_sends(array, index, s):
-        rows = tile_rows(s)
-        place, sem = array.at[mine, rows], slot_recv.at[index, mine, s]
+        odd = lax.rem(s, 2)
+        place = array.at[mine, tile_rows(s)]
         return (
-            remote(place, place, x_sem.at[index, s], sem, x_peer),
-            remote(place, place, y_sem.at[index, s], sem, y_peer),
-        )
-
-    def tile_pass(array, index, s):
+            remote(
+                place, place, slot_sem.at[0, s], slot_recv.at[index, 1 - odd, s], x_peer
+            ),
+            remote(place, place, slot_sem.at[1, s], slot_recv.at[index, odd, s], y_peer),
+        )
+
+    def tile_pass(array, index, s, kind):
         odd = lax.rem(s, 2)
         slot = behind * (1 - odd) + beside * odd
         place = array.at[slot, tile_rows(s)]
@@ -344,26 +356,28 @@
             "fs": f + (1 - odd) * (1 - 2 * x),
             "tp": lax.rem(t + 2 * odd, tp_size),
         }
-        return remote(
-            place, place, pass_sem.at[index, s], slot_recv.at[index, slot, s], device
-        )
+        return remote(place, place, slot_sem.at[2, s], slot_recv.at[index, kind, s], device)
+
+    gathered = (None, *hidden_one, second, channels, third, *hidden_two)
 
     def emit(array, index, s):
+        if index > 1:
+            for copy in tile_sends(gathered[index - 1], index - 1, s):
+                copy.wait_send()
         for copy in tile_sends(array, index, s):
             copy.start()
 
     def relay(array, index, s):
-        copy = tile_pass(array, index, s)
-        copy.wait_recv()
-        copy.start()
+        if index > 1:
+            tile_pass(gathered[index - 1], index - 1, s, 1).wait_send()
+        tile_pass(array, index, s, 0).wait_recv()
+        tile_pass(array, index, s, 1).start()
 
     def complete(array, index, s):
-        odd = lax.rem(s, 2)
-        for slot in (beside * (1 - odd) + behind * odd, corner):
-            place = array.at[slot, tile_rows(s)]
-            remote(
-                place, place, x_sem.at[index, s], slot_recv.at[index, slot, s], x_peer
-            ).wait_recv()
+        place = array.at[pl.ds(0, 2), tile_rows(s)]
+        remote(
+            place, place, slot_sem.at[0, s], slot_recv.at[index, 1, s], x_peer
+        ).wait_recv()
 
     total_rows = tokens.shape[0]
     tiles = total_rows // TILE
@@ -425,7 +439,7 @@
 
         return work
 
-    def lowered(halves, down, residual, rows):
+    def lowered(halves, down, residual, rows, columns):
         half = halves[0].shape[2]
         total = sum(
             dot(
@@ -435,12 +449,14 @@
             for k in range(tp_size)
             for part, hidden in enumerate(halves)
         )
-        value = residual[mine, rows, :].astype(jnp.float32) + 0.5 * total
+        value = residual[mine, rows, columns].astype(jnp.float32) + 0.5 * total
         return value.astype(jnp.bfloat16)
 
     def down_tile(s):
         rows = tile_rows(s)
-        second[mine, rows, :] = lowered(hidden_one, whole[2], first, rows)
+        second[mine, rows, :] = lowered(
+            hidden_one, whole[2], first, rows, slice(None)
+        )
 
     def mix_tile(s):
         rows = tile_rows(s)
@@ -460,13 +476,18 @@
             jnp.bfloat16
         )
 
-    def out_send(s):
-        rows = tile_rows(s)
-        return remote(final.at[rows], out.at[rows], out_sem.at[s], out_recv.at[s], partner)
-
-    def out_keep(s):
-        rows = tile_rows(s)
-        return pltpu.make_async_copy(final.at[rows], out.at[rows], out_sem.at[s])
+    cut = shards[7].shape[1]
+    last_columns = (slice(0, cut), slice(cut, cut + shards[8].shape[1]))
+
+    def out_send(part, rows):
+        place = (rows, last_columns[part])
+        return remote(
+            final.at[place], out.at[place], out_sem.at[part], out_recv.at[part], partner
+        )
+
+    def out_keep(part, rows):
+        place = (rows, last_columns[part])
+        return pltpu.make_async_copy(final.at[place], out.at[place], out_sem.at[part])
 
     def spread(blocks, at):
         size = blocks.shape[1]
@@ -507,25 +528,31 @@
     links.send(tokens, target, token_sem.at[3], sem, twin, away)
     settle(0, "home")
     launch(0, home)
+    launch_last(0, home)
     convert(1)
     swap(1)
     token_cross(away)
     settle(1, "home")
-    launch(1, home)
-    arrive(0, 2 * z + 1 - c, home)
+    launch_last(1, home)
+    launch(1, home & end)
+    arrive_twin(0, 1, pace_sem, home)
     token_cross(home)
     settle(0, "away")
     launch(0, away)
+    launch_last(0, away)
+    pump(0, inner & home)
+    launch(1, home & inner)
     for p in range(2, count):
         convert(p)
         swap(p)
     for p in range(2, count):
         settle(p, "home")
-        launch(p, home & end)
-    pump(0, inner & home)
+    launch(2, home & inner)
     settle(1, "away")
-    launch(1, away)
+    launch_last(1, away)
+    launch(1, away & end)
     pump(0, inner & away)
+    launch(1, away & inner)
     for k in range(2):
         slot = 2 * y + k
         token_arrive(slot, away)
@@ -544,10 +571,15 @@
     token_arrive(other, home)
     token_arrive(2 * (1 - y), home)
     token_arrive(2 * (1 - y) + 1, home)
+    for p in range(2, count):
+        launch(p, home & end)
     pump(1, inner)
     for p in range(2, 4):
         settle(p, "away")
-        launch(p, inner | away)
+        launch(p, away)
+    launch(3, home & inner)
+    launch_last(2, inner)
+    launch_last(3, inner)
     token_arrive(2 * (1 - y), away)
     token_arrive(2 * (1 - y) + 1, away)
     loop(functools.partial(norm_rows, first, pre_gain))
@@ -558,11 +590,14 @@
         launch(p, away & end)
     pump(2, inner)
     launch(4, inner)
+    launch_last(4, inner)
+    launch(5, inner)
     relay(hidden_one[0], 1, tiles - 1)
     ready(1)
     stage(2, hidden_one[1], hidden_tile(whole[1], hidden_one[1]))
     pump(3, inner)
-    launch(5, inner)
+    launch_last(5, inner)
+    launch(6, inner)
     relay(hidden_one[1], 2, tiles - 1)
     for away_copy, home_copy in side_copies():
         when(away, away_copy.wait)
@@ -573,14 +608,18 @@
     stage(3, second, down_tile, before=((1, hidden_one[0]), (2, hidden_one[1])))
     pump(4, inner)
     pump(5, inner)
-    launch(6, inner)
+    launch_last(6, inner)
+    launch(7, inner)
+    launch(8, inner)
     ready(3)
     stage(4, channels, mix_tile, earlier=(3, second), before=((3, second),))
     pump(6, inner)
-    launch(7, inner)
+    launch_last(7, inner)
+    launch_last(8, inner)
     ready(4)
     stage(5, third, out_tile, earlier=(4, channels), before=((4, channels),))
     pump(7, inner)
+    pump(8, inner)
     relay(third, 5, tiles - 1)
     ready(5)
     post_tile = hidden_tile(whole[5], hidden_two[0])
@@ -594,29 +633,41 @@
     ready(6)
     stage(7, hidden_two[1], hidden_tile(whole[6], hidden_two[1]))
     relay(hidden_two[1], 7, tiles - 1)
-    ready(7)
-
-    def last_tile(s):
-        rows = tile_rows(s)
-        complete(hidden_two[0], 6, s)
-        complete(hidden_two[1], 7, s)
-        final[rows, :] = lowered(hidden_two, whole[7], third, rows)
-        when(away, out_send(s).start)
-        when(home, out_keep(s).start)
-
-    loop(last_tile)
-    gathered = (*hidden_one, second, channels, third, *hidden_two)
+    for part, size in enumerate((2 * TILE, total_rows)):
+        ready(7 + part)
+
+        def last_rows(i, part=part, size=size):
+            rows = pl.ds(pl.multiple_of(i * size, size), size)
+            if part == 0:
+                for k in range(2):
+                    complete(hidden_two[0], 6, 2 * i + k)
+                    complete(hidden_two[1], 7, 2 * i + k)
+            final[rows, last_columns[part]] = lowered(
+                hidden_two, whole[7 + part], third, rows, last_columns[part]
+            )
+            when(away, out_send(part, rows).start)
+            when(home, out_keep(part, rows).start)
+
+        if size == total_rows:
+            last_rows(0)
+        else:
+            lax.fori_loop(0, total_rows // size, lambda i, carry: (last_rows(i), carry)[1], 0)
+
+    links.drain()
+    for (p, _), entries in taken.items():
+        for copy, condition in entries if p >= count - TAKEN else ():
+            when(condition, copy.wait_send)
 
     def drain_tiles(s):
-        for index, array in enumerate(gathered):
-            for copy in tile_sends(array, index + 1, s):
-                copy.wait_send()
-            tile_pass(array, index + 1, s).wait_send()
-        when(away, out_send(s).wait)
-        when(home, out_keep(s).wait)
-
-    links.drain()
+        for copy in tile_sends(gathered[-1], len(gathered) - 1, s):
+            copy.wait_send()
+        tile_pass(gathered[-1], len(gathered) - 1, s, 1).wait_send()
+
     loop(drain_tiles)
+    everything = pl.ds(0, total_rows)
+    for part in range(2):
+        when(away, out_send(part, everything).wait)
+        when(home, out_keep(part, everything).wait)
 
 
 def fused(
@@ -642,16 +693,17 @@
     post_down,
 ):
     matrices = [
-        pre_gate,
-        pre_up,
+        pre_gate.T,
+        pre_up.T,
         pre_down,
         branch_proj,
         gate_proj,
         out_proj,
-        post_gate,
-        post_up,
+        post_gate.T,
+        post_up.T,
         post_down,
     ]
+    last = post_down.shape[1] - 128
     shards = [
         pre_gate.shape[::-1],
         pre_gate.shape[::-1],
@@ -660,7 +712,8 @@
         out_proj.shape,
         post_gate.shape[::-1],
         post_gate.shape[::-1],
-        post_down.shape,
+        (post_down.shape[0], last),
+        (post_down.shape[0], 128),
     ]
     rows, width = tokens.shape
     hidden = pre_gate.shape[1]
@@ -685,7 +738,7 @@
         out_shape=jax.ShapeDtypeStruct(tokens.shape, tokens.dtype),
         in_specs=[pl.BlockSpec(memory_space=pltpu.VMEM)] * (5 + len(side))
         + [pl.BlockSpec(memory_space=pl.ANY)] * len(matrices),
-        out_specs=pl.BlockSpec(memory_space=OUT_SPACE),
+        out_specs=pl.BlockSpec(memory_space=pl.ANY),
         scratch_shapes=[
             *(pltpu.VMEM((fs_size * s[0], s[1]), jnp.bfloat16) for s in shards),
             *(pltpu.VMEM(s, jnp.bfloat16) for s in shards),
@@ -702,24 +755,22 @@
             pltpu.VMEM((rows, width), jnp.bfloat16),
             pltpu.VMEM((channels, 2 * channels), jnp.bfloat16),
             *(pltpu.VMEM(s.shape, s.dtype) for s in side),
-            dma((count, fs_size)),
-            dma((count, depth)),
-            dma((count, depth)),
             dma((count, depth)),
             dma((count,)),
+            dma,
+            dma((count, 3)),
+            dma((TAKEN, 3, depth)),
             dma((count,)),
             dma((len(matrices),)),
             dma((4,)),
             dma((tp_size,)),
             dma((2,)),
-            dma((8, tp_size, tiles)),
-            dma((8, tiles)),
-            dma((8, tiles)),
-            dma((8, tiles)),
+            dma((8, 2, tiles)),
+            dma((3, tiles)),
             dma((len(side),)),
             dma((len(side),)),
-            dma((tiles,)),
-            dma((tiles,)),
+            dma((2,)),
+            dma((2,)),
         ],
         compiler_params=pltpu.CompilerParams(
             collective_id=0, has_side_effects=True, vmem_limit_bytes=62 * 2**20
@@ -731,7 +782,8 @@
     shards = [a for i, a in enumerate(arrays) if i in (2, 3, 4, 6, 7, 13, 15, 16, 17)]
     rows_fit = all(a.shape[0] % 16 == 0 for a in shards)
     lanes_fit = all(arrays[i].shape[1] % 128 == 0 for i in (0, 6, 7))
-    tiles_fit = arrays[0].shape[0] % TILE == 0 and arrays[2].shape[1] % 32 == 0
+    lanes_fit = lanes_fit and arrays[17].shape[1] > 128
+    tiles_fit = arrays[0].shape[0] % (2 * TILE) == 0 and arrays[2].shape[1] % 32 == 0
     turned_fit = all(arrays[i].shape[0] % 128 == 0 for i in (2, 3, 15, 16))
     return (
         rows_fit

time: 197 us -> 184 us (0.934)
  the two profiles are of different devices: /device:TPU:13 before, /device:TPU:1 now
where the time goes in v3:
time: 184 us; the launch traced here: 183 us
  Pallas kernels  181 us (98%)
  local copies, waits for them, and re-layouts  1.87 us (1%)
    pallas_call x1, Pallas kernels, fused(): pl.pallas_call(functools.partial(layer_kernel, fs_size, tp_size), out_sha...  181 us

profile of v3, /device:TPU:1, one launch (start us, length us, event | category | flops | bytes accessed | tf_op | source)
XLA Modules:
  0.0 183.1 jit_solution(6019537073846071776)
XLA Ops:
  0.0 181.2 %shard_map.172 = bf16[512,512]{1,0:T(8,128)(2,1)} custom-call(bf16[512,512]{1,0:T(8,128)(2,1)} %refs_0_.1, f32[1,2048]{1,0:T(1,128)} %bitcast.13, f32[1,2048]{1,0:T(1,128)} %bitcast.14, f32[1,1024]{1,0:T(1,128)} %bitcast.16, f32[1,2048]{1,0:T(1,128)} %bitcast.15, f32[4,256]{1,0:T(4,128)} %refs_5_.1, f32[4,64,64]{2,1,0:T(8,128)} %refs_6_.1, ...), custom_call_target="tpu_custom_call" | custom-call | tf_op jit(solution)/shard_map/pallas_call | solution.py:736
  181.2 1.9 %copy.20 = bf16[512,512]{1,0:T(8,128)(2,1)} copy(bf16[512,512]{1,0:T(8,128)(2,1)} %shard_map.172) | data formatting | bytes 1048576

commit v4 on v3

--- a/solution.py
+++ b/solution.py
@@ -170,7 +170,7 @@
 
 
 def layer_kernel(fs_size, tp_size, *refs):
-    (tokens, pre_gain, mix_gain, channel_gain, post_gain) = refs[:5]
+    (tokens_in, pre_gain, mix_gain, channel_gain, post_gain) = refs[:5]
     own_side = refs[5:9]
     matrices = refs[9:18]
     out = refs[18]
@@ -188,6 +188,7 @@
     token_sem, token_recv, token_pass = refs[46:49]
     slot_recv, slot_sem = refs[49:51]
     side_sem, side_recv, out_sem, out_recv = refs[51:55]
+    tokens, tokens_sem = refs[55:57]
     taps, retain, admit, decay = side
 
     f = lax.axis_index("fs")
@@ -222,7 +223,11 @@
     def load(m):
         return pltpu.make_async_copy(matrices[m], raw[m], raw_sem.at[m])
 
-    for m in range(len(matrices)):
+    tokens_copy = pltpu.make_async_copy(tokens_in, tokens, tokens_sem)
+    for m in range(2):
+        load(m).start()
+    tokens_copy.start()
+    for m in range(2, len(matrices)):
         load(m).start()
 
     def convert(p):
@@ -320,12 +325,18 @@
             when(who, copy.start)
             taken.setdefault((p, key), []).append((copy, who))
 
-    def pump(p, condition):
-        for distance in range(1, depth):
+    def pump(p, condition, distances=None):
+        for distance in distances or range(1, depth):
             for sign in (-1, 1):
                 level = z + sign * distance
                 exists = (level >= 0) & (level < depth)
                 take(p, sign * distance, lax.rem(level + depth, depth), condition & exists)
+
+    def near(p):
+        pump(p, inner, (1,))
+
+    def far(p):
+        pump(p, inner, range(2, depth))
 
     def ready(p):
         pump(p, end)
@@ -343,9 +354,9 @@
         place = array.at[mine, tile_rows(s)]
         return (
             remote(
-                place, place, slot_sem.at[0, s], slot_recv.at[index, 1 - odd, s], x_peer
+                place, place, slot_sem.at[0, s], slot_recv.at[index - 1, 1 - odd, s], x_peer
             ),
-            remote(place, place, slot_sem.at[1, s], slot_recv.at[index, odd, s], y_peer),
+            remote(place, place, slot_sem.at[1, s], slot_recv.at[index - 1, odd, s], y_peer),
         )
 
     def tile_pass(array, index, s, kind):
@@ -356,7 +367,7 @@
             "fs": f + (1 - odd) * (1 - 2 * x),
             "tp": lax.rem(t + 2 * odd, tp_size),
         }
-        return remote(place, place, slot_sem.at[2, s], slot_recv.at[index, kind, s], device)
+        return remote(place, place, slot_sem.at[2, s], slot_recv.at[index - 1, kind, s], device)
 
     gathered = (None, *hidden_one, second, channels, third, *hidden_two)
 
@@ -376,7 +387,7 @@
     def complete(array, index, s):
         place = array.at[pl.ds(0, 2), tile_rows(s)]
         remote(
-            place, place, slot_sem.at[0, s], slot_recv.at[index, 1, s], x_peer
+            place, place, slot_sem.at[0, s], slot_recv.at[index - 1, 1, s], x_peer
         ).wait_recv()
 
     total_rows = tokens.shape[0]
@@ -521,6 +532,7 @@
             )
 
     swap(0)
+    tokens_copy.wait()
     keep_tokens = pltpu.make_async_copy(tokens, first.at[t], token_sem.at[0])
     when(home, keep_tokens.start)
     target, sem = first.at[t], token_recv.at[t]
@@ -535,6 +547,11 @@
     settle(1, "home")
     launch_last(1, home)
     launch(1, home & end)
+    for p in range(2, 4):
+        convert(p)
+        swap(p)
+        settle(p, "home")
+        launch_last(p, home)
     arrive_twin(0, 1, pace_sem, home)
     token_cross(home)
     settle(0, "away")
@@ -542,10 +559,10 @@
     launch_last(0, away)
     pump(0, inner & home)
     launch(1, home & inner)
-    for p in range(2, count):
+    for p in range(4, count):
         convert(p)
         swap(p)
-    for p in range(2, count):
+    for p in range(4, count):
         settle(p, "home")
     launch(2, home & inner)
     settle(1, "away")
@@ -573,32 +590,38 @@
     token_arrive(2 * (1 - y) + 1, home)
     for p in range(2, count):
         launch(p, home & end)
-    pump(1, inner)
+    near(1)
     for p in range(2, 4):
         settle(p, "away")
         launch(p, away)
     launch(3, home & inner)
-    launch_last(2, inner)
-    launch_last(3, inner)
     token_arrive(2 * (1 - y), away)
     token_arrive(2 * (1 - y) + 1, away)
     loop(functools.partial(norm_rows, first, pre_gain))
+    far(1)
+    launch_last(2, away & inner)
+    launch_last(3, away & inner)
     ready(0)
     stage(1, hidden_one[0], hidden_tile(whole[0], hidden_one[0]))
     for p in range(4, count):
         settle(p, "away")
         launch(p, away & end)
-    pump(2, inner)
+    near(2)
+    launch_last(4, inner)
     launch(4, inner)
-    launch_last(4, inner)
     launch(5, inner)
     relay(hidden_one[0], 1, tiles - 1)
+    far(2)
+    near(3)
     ready(1)
     stage(2, hidden_one[1], hidden_tile(whole[1], hidden_one[1]))
-    pump(3, inner)
+    far(3)
+    near(4)
     launch_last(5, inner)
     launch(6, inner)
     relay(hidden_one[1], 2, tiles - 1)
+    far(4)
+    near(5)
     for away_copy, home_copy in side_copies():
         when(away, away_copy.wait)
         when(home, home_copy.wait)
@@ -606,20 +629,22 @@
     spread(admit, gates.shape[0])
     ready(2)
     stage(3, second, down_tile, before=((1, hidden_one[0]), (2, hidden_one[1])))
-    pump(4, inner)
-    pump(5, inner)
+    far(5)
     launch_last(6, inner)
+    near(6)
     launch(7, inner)
     launch(8, inner)
     ready(3)
     stage(4, channels, mix_tile, earlier=(3, second), before=((3, second),))
-    pump(6, inner)
+    far(6)
     launch_last(7, inner)
     launch_last(8, inner)
+    near(7)
+    near(8)
     ready(4)
     stage(5, third, out_tile, earlier=(4, channels), before=((4, channels),))
-    pump(7, inner)
-    pump(8, inner)
+    far(7)
+    far(8)
     relay(third, 5, tiles - 1)
     ready(5)
     post_tile = hidden_tile(whole[5], hidden_two[0])
@@ -633,10 +658,11 @@
     ready(6)
     stage(7, hidden_two[1], hidden_tile(whole[6], hidden_two[1]))
     relay(hidden_two[1], 7, tiles - 1)
-    for part, size in enumerate((2 * TILE, total_rows)):
+    size = 2 * TILE
+    for part in range(2):
         ready(7 + part)
 
-        def last_rows(i, part=part, size=size):
+        def last_rows(i, part=part):
             rows = pl.ds(pl.multiple_of(i * size, size), size)
             if part == 0:
                 for k in range(2):
@@ -648,10 +674,7 @@
             when(away, out_send(part, rows).start)
             when(home, out_keep(part, rows).start)
 
-        if size == total_rows:
-            last_rows(0)
-        else:
-            lax.fori_loop(0, total_rows // size, lambda i, carry: (last_rows(i), carry)[1], 0)
+        lax.fori_loop(0, total_rows // size, lambda i, carry: (last_rows(i), carry)[1], 0)
 
     links.drain()
     for (p, _), entries in taken.items():
@@ -735,10 +758,11 @@
     stacked = lambda columns: pltpu.VMEM((tp_size, rows, columns), jnp.bfloat16)
     return pl.pallas_call(
         functools.partial(layer_kernel, fs_size, tp_size),
-        out_shape=jax.ShapeDtypeStruct(tokens.shape, tokens.dtype),
-        in_specs=[pl.BlockSpec(memory_space=pltpu.VMEM)] * (5 + len(side))
+        out_shape=pltpu.VMEM(tokens.shape, tokens.dtype),
+        in_specs=[pl.BlockSpec(memory_space=pl.ANY)]
+        + [pl.BlockSpec(memory_space=pltpu.VMEM)] * (4 + len(side))
         + [pl.BlockSpec(memory_space=pl.ANY)] * len(matrices),
-        out_specs=pl.BlockSpec(memory_space=pl.ANY),
+        out_specs=pl.BlockSpec(memory_space=pltpu.VMEM),
         scratch_shapes=[
             *(pltpu.VMEM((fs_size * s[0], s[1]), jnp.bfloat16) for s in shards),
             *(pltpu.VMEM(s, jnp.bfloat16) for s in shards),
@@ -765,12 +789,14 @@
             dma((4,)),
             dma((tp_size,)),
             dma((2,)),
-            dma((8, 2, tiles)),
+            dma((7, 2, tiles)),
             dma((3, tiles)),
             dma((len(side),)),
             dma((len(side),)),
             dma((2,)),
             dma((2,)),
+            pltpu.VMEM(tokens.shape, tokens.dtype),
+            dma,
         ],
         compiler_params=pltpu.CompilerParams(
             collective_id=0, has_side_effects=True, vmem_limit_bytes=62 * 2**20

time: 184 us -> 183 us (level)
  no operation moved by 1% of the time
where the time goes in v4:
time: 183 us
  Pallas kernels  182 us (99%)
    pallas_call x1, Pallas kernels, fused(): pl.pallas_call(functools.partial(layer_kernel, fs_size, tp_size), out_sha...  182 us

profile of v4, /device:TPU:1, one launch (start us, length us, event | category | flops | bytes accessed | tf_op | source)
XLA Modules:
  0.0 182.9 jit_solution(11919136424488080796)
XLA Ops:
  0.0 182.0 %shard_map.172 = bf16[512,512]{1,0:T(8,128)(2,1)S(1)} custom-call(bf16[512,512]{1,0:T(8,128)(2,1)} %refs_0_.1, f32[1,2048]{1,0:T(1,128)} %bitcast.13, f32[1,2048]{1,0:T(1,128)} %bitcast.14, f32[1,1024]{1,0:T(1,128)} %bitcast.16, f32[1,2048]{1,0:T(1,128)} %bitcast.15, f32[4,256]{1,0:T(4,128)} %refs_5_.1, f32[4,64,64]{2,1,0:T(8,128)} %refs_6_.1, ...), custom_call_target="tpu_custom_call" | custom-call | tf_op jit(solution)/shard_map/pallas_call | solution.py:759
  182.1 0.8 copy.20
